TPU v7x, 128 devices: a whole 4x4x4 slice. The times are simulated.
128 devices in a mesh: rep: 2 (over z_hi), fs: 32 (over z_lo, y, x), tp: 2 (over core).
Axes of the slice: x: 4, y: 4, z: 4 (z_hi: 2, z_lo: 2; z = z_hi * 2 + z_lo), core: 2. Of those that a mesh axis runs over, the one named last changes fastest.
Arguments:
- resid: bfloat16 [65536, 2048], P(('rep', 'fs'), 'tp'), may hold values from -6 to 6
- gain_mix_in: float32 [2048], replicated, may hold values from 0.1 to 1.9
- u_weight: float32 [2048, 1024], P('fs', 'tp'), may hold values from -0.125 to 0.125
- v_weight: float32 [2048, 1024], P('fs', 'tp'), may hold values from -0.125 to 0.125
- u_scale: float32 [1024], P('tp'), may hold values from 0.5 to 2
- v_scale: float32 [1024], P('tp'), may hold values from 0.3 to 3
- v_gain: float32 [1024], P('tp'), may hold values from 0.1 to 1.9
- mix_matrix: float32 [16, 128, 128], P('tp'), may hold values from -0.5 to 0.5
- mix_bias: float32 [16, 128], P('tp'), may hold values from 0.1 to 1.9
- out_weight: float32 [1024, 2048], P('tp', 'fs'), may hold values from -0.1875 to 0.1875
- out_scale: float32 [2048], P('fs'), may hold values from 0.3 to 3
- gain_mix_out: float32 [2048], replicated, may hold values from 0.1 to 1.9
- gain_ffn_in: float32 [2048], replicated, may hold values from 0.1 to 1.9
- up_weight: float32 [2048, 4096], P('fs', 'tp'), may hold values from -0.125 to 0.125
- up_scale: float32 [4096], P('tp'), may hold values from 0.5 to 2
- down_weight: float32 [4096, 2048], P('tp', 'fs'), may hold values from -0.09375 to 0.09375
- down_scale: float32 [2048], P('fs'), may hold values from 0.3 to 3
- gain_ffn_out: float32 [2048], replicated, may hold values from 0.1 to 1.9
Outputs:
- result: bfloat16 [65536, 2048], P(('rep', 'fs'), 'tp')
All inputs are finite; a program needn't handle non-finite values.
Results may differ from a plain program's by a relative error of at most 0.013.
Values may be sent and summed in bfloat16 or wider, within the bound.
A program may use at most 128 MiB of HBM per device.

v0:
```python
import jax
import jax.numpy as jnp
from jax import lax
from jax.sharding import PartitionSpec as P


def turned_gather(arrays, axis, dims):
    turned = [jnp.moveaxis(a, dim, 0) for a, dim in zip(arrays, dims)]
    widths = [t[0].size for t in turned]
    both = jnp.concatenate([t.reshape(-1, w) for t, w in zip(turned, widths)], axis=1)
    result = lax.all_gather(both, axis, axis=0, tiled=True)
    pieces = jnp.split(result, [sum(widths[:k]) for k in range(1, len(widths))], axis=1)
    return tuple(
        (
            jnp.moveaxis(b.reshape(-1, *t.shape[1:]), 0, dim)
            for b, t, dim in zip(pieces, turned, dims)
        )
    )


def in_one_piece(arrays, axis, dim, along):
    ends, at = ([], 0)
    for a in arrays[:-1]:
        at += a.shape[along]
        ends.append(at)
    both = jnp.concatenate(arrays, axis=along)
    return tuple(jnp.split(lax.all_gather(both, axis, axis=dim, tiled=True), ends, axis=along))


def copy_for_each(array, axis):
    copies = jnp.broadcast_to(array, (lax.axis_size(axis), *array.shape))
    return lax.all_to_all(copies, axis, split_axis=0, concat_axis=0, tiled=True)


def over_copies(array, axis):
    return copy_for_each(array, axis).sum(axis=0)


def packed_total(arrays, axis):
    vector, at, gathered = (jnp.concatenate([a.reshape(-1) for a in arrays]), 0, [])
    running = over_copies(vector, axis)
    for a in arrays:
        gathered.append(running[at : at + a.size].reshape(a.shape))
        at += a.size
    return tuple(gathered)


def in_order(pieces, dim):
    dims = list(pieces.shape[1:])
    dims[dim] *= pieces.shape[0]
    return jnp.moveaxis(pieces, 0, dim).reshape(dims)


def gathered_copies(array, axis, dim):
    pieces = copy_for_each(array, axis)
    return in_order(pieces, dim)


def total_of_pieces(array, axis):
    pieces = lax.all_gather(array, axis).astype(jnp.float32)
    return pieces.sum(axis=0)


def in_blocks(array, dim, peers):
    before, after = (array.shape[:dim], array.shape[dim + 1 :])
    return jnp.moveaxis(array.reshape(*before, peers, -1, *after), dim, 0)


def sent_and_summed(array, axis, dim):
    peers = lax.axis_size(axis)
    pieces = lax.all_to_all(in_blocks(array, dim, peers), axis, 0, 0, tiled=True)
    return jnp.sum(pieces.astype(jnp.float32), axis=0)


def rms_norm(values, gain, width, power_sum):
    return values * lax.rsqrt(power_sum / width + 1e-06) * gain


def local(
    resid,
    gain_mix_in,
    u_weight,
    v_weight,
    u_scale,
    v_scale,
    v_gain,
    mix_matrix,
    mix_bias,
    out_weight,
    out_scale,
    gain_mix_out,
    gain_ffn_in,
    up_weight,
    up_scale,
    down_weight,
    down_scale,
    gain_ffn_out,
):
    rows = resid.shape[0]
    part_width = resid.shape[1]
    width = part_width * lax.axis_size("tp")
    lane = lax.axis_index("tp")
    full_rows = lax.all_gather(resid, "tp", axis=1, tiled=True)
    out_scales, down_scales = turned_gather((out_scale, down_scale), "fs", (0, 0))
    full_float = full_rows.astype(jnp.float32)
    normed = rms_norm(
        full_float, gain_mix_in, width, jnp.sum(full_float * full_float, axis=1, keepdims=True)
    ).astype(jnp.bfloat16)
    branch_cols = u_weight.shape[1]
    pieces = in_one_piece(
        (u_weight.astype(jnp.bfloat16), v_weight.astype(jnp.bfloat16)), "fs", 0, 1
    )
    u_pre = jnp.dot(normed, pieces[0], preferred_element_type=jnp.float32)
    v_pre = jnp.dot(normed, pieces[1], preferred_element_type=jnp.float32)
    u_act = jax.nn.gelu(u_pre * u_scale)
    v_act = jax.nn.gelu(v_pre * v_scale)
    total, squares = packed_total(
        (jnp.sum(v_act, axis=1, keepdims=True), jnp.sum(v_act * v_act, axis=1, keepdims=True)), "tp"
    )
    branch_width = branch_cols * lax.axis_size("tp")
    centre = total / branch_width
    spread = squares / branch_width - centre * centre
    v_norm = ((v_act - centre) * lax.rsqrt(spread + 1e-06) * v_gain).astype(jnp.bfloat16)
    groups = mix_matrix.shape[0]
    block = mix_matrix.shape[1]
    blocks = v_norm.reshape(rows // block, block, groups, branch_cols // groups)
    mixed = (
        jnp.einsum(
            "gts,bsgd->btgd",
            mix_matrix.astype(jnp.bfloat16),
            blocks,
            preferred_element_type=jnp.float32,
        )
        + mix_bias.T[None, :, :, None]
    )
    gated = (u_act * mixed.reshape(rows, branch_cols)).astype(jnp.bfloat16)
    partial_value = jnp.dot(
        gated,
        gathered_copies(out_weight.astype(jnp.bfloat16), "fs", 1),
        preferred_element_type=jnp.float32,
    )
    mix_out = (
        total_of_pieces(partial_value.astype(jnp.bfloat16), "tp").astype(jnp.float32) * out_scales
    )
    power = jnp.sum(mix_out * mix_out, axis=1, keepdims=True)
    middle_full = (full_float + rms_norm(mix_out, gain_mix_out, width, power)).astype(jnp.bfloat16)
    middle = lax.dynamic_slice_in_dim(middle_full, lane * part_width, part_width, 1)
    middle_float = middle_full.astype(jnp.float32)
    ffn_in = rms_norm(
        middle_float,
        gain_ffn_in,
        width,
        jnp.sum(middle_float * middle_float, axis=1, keepdims=True),
    ).astype(jnp.bfloat16)
    up_half = up_weight.astype(jnp.bfloat16)
    down_half = down_weight.astype(jnp.bfloat16)
    whole_up = lax.all_gather(up_half, "fs", axis=0, tiled=True)
    raised = jnp.dot(ffn_in, whole_up, preferred_element_type=jnp.float32)
    hidden = jnp.square(jax.nn.relu(raised * up_scale)).astype(jnp.bfloat16)
    whole_down = lax.all_gather(down_half, "fs", axis=1, tiled=True)
    terms = jnp.dot(hidden, whole_down, preferred_element_type=jnp.float32)
    own_down = lax.dynamic_slice_in_dim(down_scales, lane * part_width, part_width, 0)
    ffn_out = sent_and_summed(terms.astype(jnp.bfloat16), "tp", 1) * own_down
    power_out = over_copies(jnp.sum(ffn_out * ffn_out, axis=1, keepdims=True), "tp")
    own_gain_out = lax.dynamic_slice_in_dim(gain_ffn_out, lane * part_width, part_width, 0)
    return (middle.astype(jnp.float32) + rms_norm(ffn_out, own_gain_out, width, power_out)).astype(
        jnp.bfloat16
    )


def solution(mesh):
    in_specs = (
        P(("rep", "fs"), "tp"),
        P(),
        P("fs", "tp"),
        P("fs", "tp"),
        P("tp"),
        P("tp"),
        P("tp"),
        P("tp", None, None),
        P("tp", None),
        P("tp", "fs"),
        P("fs"),
        P(),
        P(),
        P("fs", "tp"),
        P("tp"),
        P("tp", "fs"),
        P("fs"),
        P(),
    )
    out_specs = P(("rep", "fs"), "tp")
    return jax.shard_map(local, mesh=mesh, in_specs=in_specs, out_specs=out_specs, check_vma=False)
```

profile of v0, /device:TPU:1, one launch (start us, length us, event | category | flops | bytes accessed | tf_op | source)
XLA Modules:
  0.0 657.6 jit_solution(17726470480720936505)
XLA Ops:
  7.3 0.9 convert_element_type.62
  8.2 0.9 convert_element_type.63
  9.8 0.9 convert_element_type.67
  10.8 18.3 %all-gather.8.cloned.1.call-done = bf16[1024,2048]{1,0:T(8,128)(2,1)} async-done(((bf16[1024,1024]{1,0:T(8,128)(2,1)}), bf16[1024,2048]{1,0:T(8,128)(2,1)}) %all-gather.8.cloned.1.call-update) | async-done | bytes 4194320 | tf_op jit(solution)/shard_map/all_gather | solution.py:103
  29.0 3.1 fusion.3
  32.1 135.9 %all-gather.10.cloned.1.call-done = bf16[2048,1024]{1,0:T(8,128)(2,1)} async-done(((bf16[64,1024]{1,0:T(8,128)(2,1)}), bf16[2048,1024]{1,0:T(8,128)(2,1)}) %all-gather.10.cloned.1.call-update) | async-done | bytes 4194320 | tf_op jit(solution)/shard_map/all_gather | solution.py:27
  168.0 5.8 fusion.68
  173.8 24.0 %all_to_all.21 = f32[2,1,2048]{2,1,0:T(1,128)S(1)} all-to-all(f32[2,1,2048]{2,1,0:T(1,128)S(1)} %broadcast_in_dim.6), channel_id=1, replica_groups=mesh['rep'=2,'fs'=32,'tp'=2] {'tp'}, dimensions={0} | all-to-all | bytes 32768 | tf_op jit(solution)/shard_map/all_to_all | solution.py:32
  197.8 1.6 broadcast_in_dim.7
  199.4 7.1 %all-to-all-start.1 = ((bf16[32,512,64]{1,2,0:T(8,128)(2,1)}), bf16[32,512,64]{1,2,0:T(8,128)(2,1)}, u32[]{:S(2)}, u32[]{:S(2)}) async-start(bf16[32,512,64]{1,2,0:T(8,128)(2,1)} %broadcast_in_dim.7), calls=%async_computation.1 | async-start | bytes 4194304 | tf_op jit(solution)/shard_map/all_to_all | solution.py:32
  206.9 2.1 reshape.90
  209.1 2.4 bitcast_add_fusion
  211.5 2.7 copy.55
  214.2 3.4 reshape.91
  217.6 15.7 %all-to-all-done.1 = bf16[32,512,64]{1,2,0:T(8,128)(2,1)} async-done(((bf16[32,512,64]{1,2,0:T(8,128)(2,1)}), bf16[32,512,64]{1,2,0:T(8,128)(2,1)}, u32[]{:S(2)}, u32[]{:S(2)}) %all-to-all-start.1) | async-done | bytes 2097184 | tf_op jit(solution)/shard_map/all_to_all | solution.py:32
  233.4 10.3 %convolution_convert_fusion = bf16[1024,2048]{1,0:T(8,128)(2,1)} fusion(bf16[512,2048]{0,1:T(8,128)(2,1)} %bitcast.5, f32[1024,512]{1,0:T(8,128)S(1)} %reshape.91, bf16[2048,1024]{1,0:T(8,128)(2,1)} %all-gather.10.cloned.1.call-done, bf16[1024,2048]{1,0:T(8,128)(2,1)} %all-gather.8.cloned.1.call-done, f32[2048]{0:T(1024)S(1)} %copy-done.10, ...), kind=kOutput, calls=%fused_computation.24 | convolution fusion | flops 4311220224 | bytes 14694400 | tf_op jit(solution)/shard_map/dot_general | solution.py:137
  243.8 1.0 copy-done.3
  244.8 0.7 convert_element_type.74
  246.4 66.4 %all-gather.1 = f32[32,64,2]{1,2,0:T(2,128)S(1)} all-gather(f32[1,64,2]{1,2,0:T(2,128)S(1)} %maximum_bitcast_fusion), channel_id=1, replica_groups=mesh['rep'=2,'fs'=32,'tp'=2] {'fs'}, dimensions={0}, use_global_device_ids=true | all-gather | bytes 16896 | tf_op jit(solution)/shard_map/all_gather | solution.py:11
  313.0 9.9 %convert_reduce_fusion = f32[1024,2048]{1,0:T(8,128)} fusion(bf16[2,1024,2048]{2,1,0:T(8,128)(2,1)} %bitcast.34), kind=kLoop, calls=%fused_computation | loop fusion | flops 6291456 | bytes 16777216 | tf_op jit(solution)/shard_map/reduce_sum | solution.py:61
  322.9 4.5 multiply_reduce_fusion
  327.5 1.3 copy-done
  328.8 4.0 fusion
  332.8 82.2 %all-gather.12.cloned.1.call-done = bf16[2048,2048]{1,0:T(8,128)(2,1)} async-done(((bf16[64,2048]{1,0:T(8,128)(2,1)}), bf16[2048,2048]{1,0:T(8,128)(2,1)}) %all-gather.12.cloned.1.call-update) | async-done | bytes 8388624 | tf_op jit(solution)/shard_map/all_gather | solution.py:157
  415.0 167.9 %all-gather.14.cloned.1.call-done = bf16[2048,2048]{0,1:T(8,128)(2,1)} async-done(((bf16[2048,64]{0,1:T(8,128)(2,1)}), bf16[2048,2048]{0,1:T(8,128)(2,1)}) %all-gather.14.cloned.1.call-update) | async-done | bytes 8388624 | tf_op jit(solution)/shard_map/all_gather | solution.py:160
  582.9 25.7 %fusion.16 = bf16[1024,2048]{1,0:T(8,128)(2,1)} fusion(bf16[2048,2048]{0,1:T(8,128)(2,1)} %all-gather.14.cloned.1.call-done, bf16[2048,2048]{1,0:T(8,128)(2,1)} %all-gather.12.cloned.1.call-done, bf16[1024,2048]{1,0:T(8,128)(2,1)} %get-tuple-element.8, f32[2048]{0:T(1024)S(1)} %copy-done.11, f32[2048]{0:T(1024)S(1)} %copy-done.12, f32[1024]{0:T(1024)S(1)} %add_rsqrt_fusion.1), kind=kOutput, calls=%fused_computation.25 | convolution fusion | flops 17198743552 | bytes 25186304 | tf_op jit(solution)/shard_map/dot_general | solution.py:161
  608.5 2.6 copy.66
  611.2 27.7 %all_to_all.22 = bf16[2,1024,1024]{2,1,0:T(8,128)(2,1)S(1)} all-to-all(bf16[2,1024,1024]{2,1,0:T(8,128)(2,1)S(1)} %bitcast.33), channel_id=1, replica_groups=mesh['rep'=2,'fs'=32,'tp'=2] {'tp'}, dimensions={0} | all-to-all | bytes 8388608 | tf_op jit(solution)/shard_map/all_to_all | solution.py:71
  638.8 1.0 convert_reduce_fusion.1
  639.9 1.9 copy-done.1
  642.3 3.7 all_to_all.23
  646.1 5.0 add_convert_fusion
  (59 shorter events, 3.5 us)
Async XLA Ops:
  6.5 161.5 %copy-start.10 = (f32[2048]{0:T(1024)S(1)}, f32[2048]{0:T(1024)}, u32[]{:S(2)}) copy-start(f32[2048]{0:T(1024)} %param.19) | copy-start | bytes 24580
  6.5 161.5 %copy-start.13 = (f32[512]{0:T(512)S(1)}, f32[512]{0:T(512)}, u32[]{:S(2)}) copy-start(f32[512]{0:T(512)} %param.23) | copy-start | bytes 6148
  6.5 22.5 %all-gather.8.cloned.1.call-start = ((), (), s32[]{:S(2)}) async-start(), calls=%async_computation.4 | async-start | bytes 6291456 | tf_op jit(solution)/shard_map/all_gather | solution.py:103
  7.3 160.7 %all-gather.10.cloned.1.call-start = ((), (), s32[]{:S(2)}) async-start(), calls=%async_computation.5 | async-start | bytes 4325376 | tf_op jit(solution)/shard_map/all_gather | solution.py:27
  173.8 32.8 %copy-start.7 = (f32[512]{0:T(512)S(1)}, f32[512]{0:T(512)}, u32[]{:S(2)}) copy-start(f32[512]{0:T(512)} %param.24) | copy-start | bytes 6148
  199.4 34.0 %all-to-all-start.1 = ((bf16[32,512,64]{1,2,0:T(8,128)(2,1)}), bf16[32,512,64]{1,2,0:T(8,128)(2,1)}, u32[]{:S(2)}, u32[]{:S(2)}) async-start(bf16[32,512,64]{1,2,0:T(8,128)(2,1)} %broadcast_in_dim.7), calls=%async_computation.1 | async-start | bytes 4194304 | tf_op jit(solution)/shard_map/all_to_all | solution.py:32
  206.5 2.6 copy-start.6
  206.5 106.5 %all-gather.16.cloned.1.call-start = ((), (), s32[]{:S(2)}) async-start(), calls=%async_computation.8 | async-start | bytes 12582912 | tf_op jit(solution)/shard_map/all_gather | solution.py:60
  214.2 19.2 %copy-start.14 = (f32[512]{0:T(512)S(1)}, f32[512]{0:T(512)}, u32[]{:S(2)}) copy-start(f32[512]{0:T(512)} %param.22) | copy-start | bytes 6148
  243.7 1.0 copy-start.3
  243.7 1.9 copy-start.4
  243.7 2.6 copy-start.8
  243.7 2.6 copy-start.9
  243.8 171.2 %all-gather.12.cloned.1.call-start = ((), (), s32[]{:S(2)}) async-start(), calls=%async_computation.6 | async-start | bytes 8650752 | tf_op jit(solution)/shard_map/all_gather | solution.py:157
  245.5 337.3 %all-gather.14.cloned.1.call-start = ((), (), s32[]{:S(2)}) async-start(), calls=%async_computation.7 | async-start | bytes 8650752 | tf_op jit(solution)/shard_map/all_gather | solution.py:160
  313.0 14.5 %copy-start.2 = (bf16[1024,2048]{1,0:T(8,128)(2,1)S(1)}, bf16[1024,2048]{1,0:T(8,128)(2,1)}, u32[]{:S(2)}) copy-start(bf16[1024,2048]{1,0:T(8,128)(2,1)} %all-gather.8.cloned.1.call-done) | copy-start | bytes 12582916
  322.9 5.9 copy-start
  322.9 5.9 copy-start.5
  328.8 254.1 %copy-start.11 = (f32[2048]{0:T(1024)S(1)}, f32[2048]{0:T(1024)}, u32[]{:S(2)}) copy-start(f32[2048]{0:T(1024)} %param.32) | copy-start | bytes 24580
  328.8 254.1 %copy-start.12 = (f32[2048]{0:T(1024)S(1)}, f32[2048]{0:T(1024)}, u32[]{:S(2)}) copy-start(f32[2048]{0:T(1024)} %param.30) | copy-start | bytes 24580
  639.9 1.9 copy-start.1
  639.9 6.2 dynamic-slice-start
Sparse Core Ops, SparseCore 0:
  9.0 19.9 all-gather.7
  30.7 137.2 all-gather.9
  243.9 22.8 all-gather.15
  268.3 146.6 all-gather.11
  416.4 166.3 all-gather.13
where the time goes:
time: 658 us
  waiting for transfers between devices  421 us (64%)
  blocking collectives  122 us (19%)
  matrix products  44.2 us (7%)
  other arithmetic  33.3 us (5%)
  local copies, waits for them, and re-layouts  16.9 us (3%)
  between operations  13.4 us (2%)
  starting transfers between devices  7.24 us (1%)
    all_gather x1, waiting for transfers between devices, local(): whole_down = lax.all_gather(down_half, 'fs', axis=1, tiled=True)  168 us
    all_gather x1, waiting for transfers between devices, in_one_piece(): lax.all_gather(both, axis, axis=dim, tiled=True)  136 us
    all_gather x1, waiting for transfers between devices, local(): whole_up = lax.all_gather(up_half, 'fs', axis=0, tiled=True)  82.2 us
    all_gather x1, blocking collectives, turned_gather(): result = lax.all_gather(both, axis, axis=0, tiled=True)  66.4 us
    all_to_all x2, blocking collectives, copy_for_each(): return lax.all_to_all(copies, axis, split_axis=0, concat_axis=0, tiled=True)  27.7 us
    all_to_all x1, blocking collectives, sent_and_summed(): lax.all_to_all(in_blocks(array, dim, peers), axis, 0, 0, tiled=True)  27.7 us
    dot_general x1, matrix products, local(): terms = jnp.dot(hidden, whole_down, preferred_element_type=jnp.float32)  25.7 us
    all_gather x1, waiting for transfers between devices, local(): full_rows = lax.all_gather(resid, 'tp', axis=1, tiled=True)  18.3 us
  transfers between devices with their start and end apart: 6, of which 5 were waited for; matrix products, arithmetic and copies ran while one was open for 6% of the time, Pallas kernels for 0%

commit v1 on v0

v1 whole, which is shorter than its diff:
```python
import functools

import jax
import jax.numpy as jnp
from jax import lax
from jax.experimental import pallas as pl
from jax.experimental.pallas import tpu as pltpu
from jax.sharding import PartitionSpec as P

MESH = pl.DeviceIdType.MESH
BF = jnp.bfloat16
F32 = jnp.float32

ROWS = 1024
WIDTH = 2048
HALF = 1024
COLS = 512
NCH = 11
STEPS = 5
SHARDS = 32
TILE = 16
GROUPS_OF_ROWS = 4
RB = 256
NRB = ROWS // RB
EB = 32

ORDERS = (
    (
        ("QY", "PY", "O", "QX", "PX"),
        ("QY", "PX", "PY", "QX", "O"),
        ("PX", "QX", "S", "PY", "QY"),
        ("PX", "QY", "QX", "PY", "S"),
    ),
    (
        ("PX", "QX", "QY", "PY", "S"),
        ("QX", "QY", "S", "PY", "PX"),
        ("QY", "PX", "PY", "QX", "O"),
        ("PY", "O", "PX", "QX", "QY"),
    ),
)
SCALE_ORDER = ("PX", "QY", "QX", "PY", "S")


def link_bits(fs):
    x, y, z = fs % 4, (fs // 4) % 4, fs // 16
    return {
        "PX": (x + x // 2) % 2,
        "QX": x // 2,
        "PY": (y + y // 2) % 2,
        "QY": y // 2,
        "S": z,
        "O": z,
    }


def place(order, fs):
    bits = link_bits(fs)
    return sum(bits[name] * (1 << k) for k, name in enumerate(order))


def order_of(c, r):
    return ORDERS[c % 2][r]


def block_rows(c, first, count):
    out = []
    for s in range(first, first + count):
        for r in range(GROUPS_OF_ROWS):
            out.append((r, place(order_of(c, r), s)))
    return out


def gathered_rows(buf, c, first=0, count=SHARDS):
    return jnp.concatenate([buf[c, r, p] for r, p in block_rows(c, first, count)], axis=0)


def dot_nt(a, b):
    return lax.dot_general(a, b, (((1,), (1,)), ((), ())), preferred_element_type=F32)


def kernel(
    pieces,
    resid,
    own_scales,
    gain_in,
    gain_out,
    gain_up,
    gain_last,
    u_scale,
    v_scale,
    v_gain,
    mix_matrix,
    bias,
    up_scale,
    result,
    buf,
    sbuf,
    scales,
    xfull,
    nbuf,
    acc,
    vn,
    gated,
    part,
    part_in,
    mid,
    hid,
    terms,
    terms_in,
    stats,
    stats_in,
    load_sem,
    send_sem,
    recv_sem,
    s_send,
    s_recv,
    x_sem,
    pair_send,
    pair_recv,
    out_sem,
):
    rep, fs, lane = lax.axis_index("rep"), lax.axis_index("fs"), lax.axis_index("tp")
    x, y, z = fs % 4, (fs // 4) % 4, fs // 16
    here = z * 16 + y * 4
    far = (1 - z) * 16 + y * 4 + x
    peer = {
        "PX": (rep, here + x + 1 - 2 * (x % 2), lane),
        "QX": (rep, here + 3 - x, lane),
        "PY": (rep, z * 16 + (y + 1 - 2 * (y % 2)) * 4 + x, lane),
        "QY": (rep, z * 16 + (3 - y) * 4 + x, lane),
        "S": (rep, far, lane),
        "O": (1 - rep, far, lane),
    }
    partner = (rep, fs, 1 - lane)
    places = {o: place(o, fs) for o in set_of_orders()}

    for c in range(NCH):
        for r in range(GROUPS_OF_ROWS):
            pltpu.make_async_copy(
                pieces.at[c, r], buf.at[c, r, places[order_of(c, r)]], load_sem.at[c]
            ).start()
    pltpu.make_async_copy(own_scales, sbuf.at[places[SCALE_ORDER]], load_sem.at[NCH]).start()
    own_x = pltpu.make_async_copy(resid, xfull.at[lane], x_sem.at[0])
    own_x.start()

    barrier = pltpu.get_barrier_semaphore()
    for device in (*peer.values(), partner):
        pl.semaphore_signal(barrier, inc=1, device_id=device, device_id_type=MESH)
    pl.semaphore_wait(barrier, 7)

    other_x = pltpu.make_async_remote_copy(
        src_ref=resid,
        dst_ref=xfull.at[lane],
        send_sem=x_sem.at[1],
        recv_sem=x_sem.at[2],
        device_id=partner,
        device_id_type=MESH,
    )
    other_x.start()

    def send(c, k):
        size = 1 << k
        for r in range(GROUPS_OF_ROWS):
            order = order_of(c, r)
            base = (places[order] // size) * size
            block = buf.at[c, r, pl.ds(base, size)]
            pltpu.make_async_remote_copy(
                src_ref=block,
                dst_ref=block,
                send_sem=send_sem.at[c],
                recv_sem=recv_sem.at[c, k],
                device_id=peer[order[k]],
                device_id_type=MESH,
            ).start()

    def arrived(c, k):
        block = buf.at[c, :, pl.ds(0, 1 << k)]
        pltpu.make_async_copy(block, block, recv_sem.at[c, k]).wait()

    def loaded(c):
        block = buf.at[c, :, 0]
        pltpu.make_async_copy(block, block, load_sem.at[c]).wait()

    def send_scales(k):
        size = 1 << k
        base = (places[SCALE_ORDER] // size) * size
        block = sbuf.at[pl.ds(base, size)]
        pltpu.make_async_remote_copy(
            src_ref=block,
            dst_ref=block,
            send_sem=s_send.at[k],
            recv_sem=s_recv.at[k],
            device_id=peer[SCALE_ORDER[k]],
            device_id_type=MESH,
        ).start()

    def scales_arrived(k):
        block = sbuf.at[pl.ds(0, 1 << k)]
        pltpu.make_async_copy(block, block, s_recv.at[k]).wait()

    def substep(t, k):
        c = t - k
        if 0 <= c < NCH:
            if k == 0:
                loaded(c)
            else:
                arrived(c, k - 1)
            send(c, k)

    def to_partner(src, dst, index):
        return pltpu.make_async_remote_copy(
            src_ref=src,
            dst_ref=dst,
            send_sem=pair_send.at[index],
            recv_sem=pair_recv.at[index],
            device_id=partner,
            device_id_type=MESH,
        )

    def x_normed():
        own_x.wait()
        other_x.wait()
        def body(i, _):
            rows = pl.ds(pl.multiple_of(i * EB, EB), EB)
            a = xfull[0, rows, :].astype(F32)
            b = xfull[1, rows, :].astype(F32)
            power = jnp.sum(a * a, axis=1, keepdims=True) + jnp.sum(b * b, axis=1, keepdims=True)
            inv = lax.rsqrt(power / WIDTH + 1e-06)
            nbuf[rows, :HALF] = (a * inv * gain_in[:, :HALF]).astype(BF)
            nbuf[rows, HALF:] = (b * inv * gain_in[:, HALF:]).astype(BF)
            return 0
        lax.fori_loop(0, ROWS // EB, body, 0)

    def row_block(i):
        return pl.ds(pl.multiple_of(i * RB, RB), RB)

    def u_part(first, last):
        def body(i, _):
            rows = row_block(i)
            w = gathered_rows(buf, 0)
            pre = jnp.dot(nbuf[rows, :], w, preferred_element_type=F32)
            acc[rows, :COLS] = jax.nn.gelu(pre * u_scale[...])
            return 0
        lax.fori_loop(first, last, body, 0)

    def v_part(first, last):
        def body(i, _):
            rows = row_block(i)
            w = gathered_rows(buf, 1)
            pre = jnp.dot(nbuf[rows, :], w, preferred_element_type=F32)
            act = jax.nn.gelu(pre * v_scale[...])
            acc[rows, COLS : 2 * COLS] = act
            total = jnp.sum(act, axis=1, keepdims=True)
            off = act - total / COLS
            spread = jnp.sum(off * off, axis=1, keepdims=True)
            lanes = lax.broadcasted_iota(jnp.int32, (RB, 128), 1)
            stats[0, rows, :] = jnp.where(lanes == 0, total, spread)
            return 0
        lax.fori_loop(first, last, body, 0)

    def v_normed(first, last):
        def body(i, _):
            rows = pl.ds(pl.multiple_of(i * EB, EB), EB)
            act = acc[rows, COLS : 2 * COLS]
            own, other = stats[0, rows, :], stats_in[0, rows, :]
            total = own[:, 0:1] + other[:, 0:1]
            apart = (own[:, 0:1] - other[:, 0:1]) / COLS
            spread = own[:, 1:2] + other[:, 1:2] + apart * apart * (COLS / 2)
            centre = total / (2 * COLS)
            inv = lax.rsqrt(spread / (2 * COLS) + 1e-06)
            vn[rows, :] = ((act - centre) * inv * v_gain[...]).astype(BF)
            return 0
        lax.fori_loop(first, last, body, 0)

    def mixing():
        def body(i, _):
            pair = i // 2
            top = pl.multiple_of((i % 2) * 512, 512)
            lanes = pl.ds(pl.multiple_of(pair * 128, 128), 128)
            m = mix_matrix[pl.ds(pair * 2, 2)].astype(BF).reshape(256, 128)
            v = jnp.concatenate(
                [vn[pl.ds(top + b * 128, 128), lanes] for b in range(4)], axis=1
            )
            both = jnp.dot(m, v, preferred_element_type=F32)
            low = lax.broadcasted_iota(jnp.int32, (128, 128), 1) < 64
            for b in range(4):
                rows = pl.ds(top + b * 128, 128)
                at = slice(b * 128, (b + 1) * 128)
                mixed = jnp.where(low, both[:128, at], both[128:, at]) + bias[:, lanes]
                gated[rows, lanes] = (acc[rows, lanes] * mixed).astype(BF)
            return 0
        lax.fori_loop(0, 8, body, 0)

    def out_part(first, last):
        for q in range(4):
            def body(i, _):
                rows = row_block(i)
                w = gathered_rows(buf, 2, q * 8, 8)
                part[rows, q * 512 : (q + 1) * 512] = dot_nt(gated[rows, :], w).astype(BF)
                return 0
            lax.fori_loop(first, last, body, 0)

    def spread_scales():
        low = lax.broadcasted_iota(jnp.int32, (1, 128), 1) < 64
        for s in range(0, SHARDS, 2):
            a, b = sbuf[place(SCALE_ORDER, s)], sbuf[place(SCALE_ORDER, s + 1)]
            at = slice(s * 64, s * 64 + 128)
            scales[0:1, at] = jnp.where(low, a, pltpu.roll(b, 64, 1))
            scales[1:2, at] = jnp.where(low, pltpu.roll(a, 64, 1), b)

    def middle(first, last):
        def body(i, _):
            rows = pl.ds(pl.multiple_of(i * EB, EB), EB)
            mix = (part[rows, :].astype(F32) + part_in[rows, :].astype(F32)) * scales[0:1, :]
            inv = lax.rsqrt(jnp.sum(mix * mix, axis=1, keepdims=True) / WIDTH + 1e-06)
            x_all = jnp.concatenate(
                [xfull[0, rows, :].astype(F32), xfull[1, rows, :].astype(F32)], axis=1
            )
            value = (x_all + mix * inv * gain_out[...]).astype(BF)
            xfull[0, rows, :] = value[:, :HALF]
            xfull[1, rows, :] = value[:, HALF:]
            wide = value.astype(F32)
            power = jnp.sum(wide * wide, axis=1, keepdims=True)
            nbuf[rows, :] = (wide * lax.rsqrt(power / WIDTH + 1e-06) * gain_up[...]).astype(BF)
            return 0
        lax.fori_loop(first, last, body, 0)

    def up_part(j, first, last):
        def body(i, _):
            rows = row_block(i)
            w = gathered_rows(buf, 3 + 2 * j)
            raised = jnp.dot(nbuf[rows, :], w, preferred_element_type=F32)
            raised = jnp.maximum(raised * up_scale[:, j * COLS : (j + 1) * COLS], 0.0)
            hid[rows, :] = (raised * raised).astype(BF)
            return 0
        lax.fori_loop(first, last, body, 0)

    def down_part(j, first, last):
        for q in range(4):
            def body(i, _):
                rows = row_block(i)
                w = gathered_rows(buf, 4 + 2 * j, q * 8, 8)
                at = slice(q * 512, (q + 1) * 512)
                term = dot_nt(hid[rows, :], w)
                acc[rows, at] = term if j == 0 else acc[rows, at] + term
                return 0
            lax.fori_loop(first, last, body, 0)

    own_cols = pl.ds(pl.multiple_of(lane * HALF, HALF), HALF)
    other_cols = pl.ds(pl.multiple_of((1 - lane) * HALF, HALF), HALF)

    def halves(i):
        def body(n, _):
            rows = pl.ds(pl.multiple_of(i * RB + n * EB, EB), EB)
            terms[rows, :] = acc[rows, other_cols].astype(BF)
            return 0
        lax.fori_loop(0, RB // EB, body, 0)

    def total_out(i):
        def body(n, _):
            rows = pl.ds(pl.multiple_of(i * RB + n * EB, EB), EB)
            own = acc[rows, own_cols].astype(BF).astype(F32)
            value = (own + terms_in[rows, :].astype(F32)) * scales[1:2, own_cols]
            acc[rows, own_cols] = value
            power = jnp.sum(value * value, axis=1, keepdims=True)
            stats[1, rows, :] = jnp.broadcast_to(power, (EB, 128))
            return 0
        lax.fori_loop(0, RB // EB, body, 0)

    def last_norm(i):
        def body(n, _):
            rows = pl.ds(pl.multiple_of(i * RB + n * EB, EB), EB)
            power = stats[1, rows, 0:1] + stats_in[1, rows, 0:1]
            inv = lax.rsqrt(power / WIDTH + 1e-06)
            value = acc[rows, own_cols] * inv * gain_last[:, own_cols]
            mid[rows, :] = (xfull[lane, rows, :].astype(F32) + value).astype(BF)
            return 0
        lax.fori_loop(0, RB // EB, body, 0)

    pending = []

    def exchange(src, dst, index):
        copy = to_partner(src, dst, index)
        copy.start()
        pending.append(copy)
        return copy

    waits = {}

    def stats_send():
        waits["stats"] = exchange(stats.at[0], stats_in.at[0], 0)

    def part_send(i):
        rows = pl.ds(i * RB, RB)
        waits["part", i] = exchange(part.at[rows], part_in.at[rows], 1 + i)

    def out_and_send(first, last):
        out_part(first, last)
        for i in range(first, last):
            part_send(i)

    def middle_of(first, last):
        for i in range(first, last):
            waits["part", i].wait_recv()
            middle(i * (RB // EB), (i + 1) * (RB // EB))

    def v_mixed():
        waits["stats"].wait_recv()
        v_normed(0, ROWS // EB)

    def compute(t):
        c = t - 6
        if c < 0:
            return {
                1: [(lambda: scales_step(t))],
                3: [x_normed] if t == 2 else [],
            }
        first, second = [], []
        if c == 0:
            first.append(lambda: arrived(0, 4))
            first.append(lambda: u_part(0, 2))
            second.append(lambda: u_part(2, 4))
        elif c == 1:
            first.append(lambda: arrived(1, 4))
            first.append(lambda: v_part(0, 2))
            second.append(lambda: v_part(2, 4))
            second.append(stats_send)
        elif c == 2:
            first.append(lambda: v_mixed())
            first.append(mixing)
            second.append(lambda: arrived(2, 4))
            second.append(lambda: out_and_send(0, 2))
            second.append(lambda: out_and_send(2, 4))
        elif c == 3:
            first.append(lambda: middle_of(0, 4))
            second.append(lambda: arrived(3, 4))
            second.append(lambda: up_part(0, 0, 4))
        elif c % 2 == 1:
            j = (c - 3) // 2
            first.append(lambda: arrived(c, 4))
            first.append(lambda: up_part(j, 0, 2))
            second.append(lambda: up_part(j, 2, 4))
        elif c < NCH - 1:
            j = (c - 4) // 2
            first.append(lambda: arrived(c, 4))
            first.append(lambda: down_part(j, 0, 2))
            second.append(lambda: down_part(j, 2, 4))
        return {1: first, 3: second}

    def scales_step(t):
        if t < STEPS:
            if t == 0:
                block = sbuf.at[0]
                pltpu.make_async_copy(block, block, load_sem.at[NCH]).wait()
            else:
                scales_arrived(t - 1)
            send_scales(t)
        else:
            scales_arrived(STEPS - 1)
            spread_scales()

    for t in range(NCH + 5):
        work = compute(t)
        for k in range(STEPS):
            substep(t, k)
            for job in work.get(k, []):
                job()

    arrived(NCH - 1, 4)
    for i in range(NRB):
        down_part(3, i, i + 1)
        halves(i)
        rows = pl.ds(i * RB, RB)
        waits["terms", i] = exchange(terms.at[rows], terms_in.at[rows], 5 + i)
    for i in range(NRB):
        waits["terms", i].wait_recv()
        total_out(i)
        rows = pl.ds(i * RB, RB)
        waits["power", i] = exchange(stats.at[1, rows], stats_in.at[1, rows], 9 + i)
    outs = []
    for i in range(NRB):
        waits["power", i].wait_recv()
        last_norm(i)
        rows = pl.ds(i * RB, RB)
        copy = pltpu.make_async_copy(mid.at[rows], result.at[rows], out_sem.at[i])
        copy.start()
        outs.append(copy)
    for copy in outs:
        copy.wait()
    for copy in pending:
        copy.wait_send()
    for c in range(NCH):
        block = buf.at[c, :, pl.ds(0, 31)]
        pltpu.make_async_copy(block, block, send_sem.at[c]).wait()
    for k in range(STEPS):
        block = sbuf.at[pl.ds(0, 1 << k)]
        pltpu.make_async_copy(block, block, s_send.at[k]).wait()


def set_of_orders():
    return sorted({*ORDERS[0], *ORDERS[1], SCALE_ORDER})


def local(
    resid,
    gain_mix_in,
    u_weight,
    v_weight,
    u_scale,
    v_scale,
    v_gain,
    mix_matrix,
    mix_bias,
    out_weight,
    out_scale,
    gain_mix_out,
    gain_ffn_in,
    up_weight,
    up_scale,
    down_weight,
    down_scale,
    gain_ffn_out,
):
    up = up_weight.reshape(64, 4, COLS).transpose(1, 0, 2)
    down = down_weight.T.reshape(64, 4, COLS).transpose(1, 0, 2)
    inner = jnp.stack([up, down], axis=1).reshape(8, 64, COLS)
    chunks = jnp.concatenate([jnp.stack([u_weight, v_weight, out_weight.T]), inner]).astype(BF)
    pieces = chunks.reshape(NCH, GROUPS_OF_ROWS, TILE, COLS)
    own_scales = jnp.concatenate([out_scale, down_scale]).reshape(1, 128)
    bias = jnp.repeat(mix_bias.T, 64, axis=1)
    row = lambda a: a.reshape(1, -1)
    vmem = pl.BlockSpec(memory_space=pltpu.VMEM)
    hbm = pl.BlockSpec(memory_space=pl.ANY)
    dma = pltpu.SemaphoreType.DMA
    return pl.pallas_call(
        kernel,
        out_shape=jax.ShapeDtypeStruct((ROWS, HALF), BF),
        in_specs=[hbm, hbm, hbm] + [vmem] * 10,
        out_specs=hbm,
        scratch_shapes=[
            pltpu.VMEM((NCH, GROUPS_OF_ROWS, SHARDS, TILE, COLS), BF),
            pltpu.VMEM((SHARDS, 1, 128), F32),
            pltpu.VMEM((2, WIDTH), F32),
            pltpu.VMEM((2, ROWS, HALF), BF),
            pltpu.VMEM((ROWS, WIDTH), BF),
            pltpu.VMEM((ROWS, WIDTH), F32),
            pltpu.VMEM((ROWS, COLS), BF),
            pltpu.VMEM((ROWS, COLS), BF),
            pltpu.VMEM((ROWS, WIDTH), BF),
            pltpu.VMEM((ROWS, WIDTH), BF),
            pltpu.VMEM((ROWS, HALF), BF),
            pltpu.VMEM((ROWS, COLS), BF),
            pltpu.VMEM((ROWS, HALF), BF),
            pltpu.VMEM((ROWS, HALF), BF),
            pltpu.VMEM((2, ROWS, 128), F32),
            pltpu.VMEM((2, ROWS, 128), F32),
            dma((NCH + 1,)),
            dma((NCH,)),
            dma((NCH, STEPS)),
            dma((STEPS,)),
            dma((STEPS,)),
            dma((3,)),
            dma((13,)),
            dma((13,)),
            dma((NRB,)),
        ],
        compiler_params=pltpu.CompilerParams(
            collective_id=0, has_side_effects=True, vmem_limit_bytes=67043328
        ),
    )(
        pieces,
        resid,
        own_scales,
        row(gain_mix_in),
        row(gain_mix_out),
        row(gain_ffn_in),
        row(gain_ffn_out),
        row(u_scale),
        row(v_scale),
        row(v_gain),
        mix_matrix,
        bias,
        row(up_scale),
    )


def solution(mesh):
    in_specs = (
        P(("rep", "fs"), "tp"),
        P(),
        P("fs", "tp"),
        P("fs", "tp"),
        P("tp"),
        P("tp"),
        P("tp"),
        P("tp", None, None),
        P("tp", None),
        P("tp", "fs"),
        P("fs"),
        P(),
        P(),
        P("fs", "tp"),
        P("tp"),
        P("tp", "fs"),
        P("fs"),
        P(),
    )
    out_specs = P(("rep", "fs"), "tp")
    return jax.shard_map(local, mesh=mesh, in_specs=in_specs, out_specs=out_specs, check_vma=False)
```

time: 658 us -> 143 us (0.22)
  waiting for transfers between devices: 421 us -> 0 us
  Pallas kernels: 0 us -> 132 us
  blocking collectives: 122 us -> 0 us
  matrix products: 44.2 us -> 0 us
  other arithmetic: 33.3 us -> 6.21 us
  between operations: 13.4 us -> 0.06 us
  local copies, waits for them, and re-layouts: 16.9 us -> 4.7 us
  starting transfers between devices: 7.24 us -> 0 us
    all_gather x5 -> x0, waiting for transfers between devices: 404 us -> none  [the longest x1 168 us: local(): whole_down = lax.all_gather(down_half, 'fs', axis=1, tiled=True)]
    pallas_call x0 -> x1, Pallas kernels: none -> 132 us  [local(): pl.pallas_call(kernel, out_shape=jax.ShapeDtypeStruct((ROWS, HALF), BF),...]
    all_gather x1 -> x0, blocking collectives: 66.4 us -> none  [turned_gather(): result = lax.all_gather(both, axis, axis=0, tiled=True)]
    all_to_all x3 -> x0, blocking collectives: 55.4 us -> none  [the longest x2 27.7 us: copy_for_each(): return lax.all_to_all(copies, axis, split_axis=0, concat_axis=0, tiled=True)]
    dot_general x4 -> x0, matrix products: 44.2 us -> none  [the longest x1 25.7 us: local(): terms = jnp.dot(hidden, whole_down, preferred_element_type=jnp.float32)]
    reduce_sum x8 -> x0, other arithmetic: 23.1 us -> none  [the longest x1 9.94 us: total_of_pieces(): return pieces.sum(axis=0)]
    all_to_all x1 -> x0, waiting for transfers between devices: 15.7 us -> none  [copy_for_each(): return lax.all_to_all(copies, axis, split_axis=0, concat_axis=0, tiled=True)]
    reshape x4 -> x1, local copies, waits for them, and re-layouts: 10.9 us -> 0.87 us  [local(): bias = jnp.repeat(mix_bias.T, 64, axis=1)]
  transfers between devices with their start and end apart: 6 -> 0, of which waited for: 5 -> 0; matrix products, arithmetic and copies ran while one was open for 6% -> 0% of each run, Pallas kernels for 0% -> 0%
where the time goes in v1:
time: 143 us
  Pallas kernels  132 us (92%)
  other arithmetic  6.21 us (4%)
  local copies, waits for them, and re-layouts  4.7 us (3%)
    pallas_call x1, Pallas kernels, local(): pl.pallas_call(kernel, out_shape=jax.ShapeDtypeStruct((ROWS, HALF), BF),...  132 us
    another operation x5, other arithmetic  3.85 us
    unnamed x3, local copies, waits for them, and re-layouts  3.08 us

profile of v1, /device:TPU:1, one launch (start us, length us, event | category | flops | bytes accessed | tf_op | source)
XLA Modules:
  0.0 142.6 jit_solution(1654492189287374387)
XLA Ops:
  0.0 0.0 copy-start
  0.0 1.4 maximum_bitcast_fusion.own_scales
  1.4 0.9 convert.28
  2.3 0.9 convert.29
  3.2 0.9 convert.30
  4.2 0.7 broadcast_in_dim.3
  4.9 0.9 copy.24.bias
  5.7 1.1 convert.31
  6.8 0.0 copy-done
  6.9 0.1 pad_maximum_fusion.1
  7.0 0.9 pad_maximum_fusion.pieces
  7.9 131.7 %shard_map.172 = bf16[1024,1024]{1,0:T(8,128)(2,1)} custom-call(bf16[11,4,16,512]{3,2,1,0:T(8,128)(2,1)} %pad_maximum_fusion.pieces, bf16[1024,1024]{1,0:T(8,128)(2,1)} %resid.1, f32[1,128]{1,0:T(1,128)} %maximum_bitcast_fusion.own_scales, f32[1,2048]{1,0:T(1,128)} %bitcast.40, f32[1,2048]{1,0:T(1,128)} %bitcast.41, f32[1,2048]{1,0:T(1,128)} %bitcast.42, ...), custom_call_target="tpu_custom_call" | custom-call | tf_op jit(solution)/shard_map/pallas_call | solution.py:535
  139.6 3.1 %copy.30 = bf16[1024,1024]{1,0:T(8,128)(2,1)} copy(bf16[1024,1024]{1,0:T(8,128)(2,1)} %shard_map.172) | data formatting | bytes 4194304
  (2 shorter events, 0.1 us)
Async XLA Ops:
  0.0 6.8 %copy-start = (f32[2048,64]{0,1:T(8,128)S(1)}, f32[2048,64]{0,1:T(8,128)}, u32[]{:S(2)}) copy-start(f32[2048,64]{0,1:T(8,128)} %param.33) | copy-start | bytes 1572868

commit v2 on v1

v2 whole, which is shorter than its diff:
```python
import itertools

import jax
import jax.numpy as jnp
from jax import lax
from jax.experimental import pallas as pl
from jax.experimental.pallas import tpu as pltpu
from jax.sharding import PartitionSpec as P

MESH = pl.DeviceIdType.MESH
BF = jnp.bfloat16
F32 = jnp.float32

ROWS = 1024
WIDTH = 2048
HALF = 1024
COLS = 512
NCH = 11
STEPS = 5
SHARDS = 32
TILE = 16
PARTS = 4
RB = 256
NRB = ROWS // RB
MB = 512
EB = 32

CROSSINGS = [
    order
    for z in ("S", "O")
    for order in itertools.permutations(("PX", "QX", "PY", "QY", z))
]
ORDERS = (
    (24, 123, 198, 39),
    (88, 195, 178, 80),
    (49, 95, 150, 78),
    (197, 183, 132, 126),
    (78, 36, 111, 7),
    (182, 153, 108, 63),
    (12, 129, 27, 66),
    (5, 173, 194, 192),
    (12, 142, 48, 111),
    (42, 75, 156, 158),
    (76, 12, 35, 169),
)
SCALE_ORDER = ("PX", "QY", "QX", "PY", "S")
PROGRAM = (
    0, 1, 2, 3, 20, 21, 22, 23, 40, 41, 42, 43, 61, 62, 63, 81, 82, 83, 100, 101,
    102, 103, 120, 60, 121, 122, 123, 140, 141, 163, 180, 182, 160, 80, 162, 183, 161, 142, 203, 202,
    201, 143, 181, 200, 4, 5, 6, 26, 7, 66, 24, 86, 44, 46, 25, 65, 67, 27, 45, 85,
    87, 126, 47, 127, 184, 64, 144, 104, 145, 105, 165, 84, 146, 107, 106, 147, 124, 125, 28, 166,
    9, 8, 48, 220, 10, 30, 70, 164, 221, 11, 50, 68, 69, 130, 222, 29, 51, 71, 109, 148,
    149, 223, 31, 32, 90, 52, 129, 49, 13, 91, 12, 14, 15, 108, 34, 73, 111, 54, 134, 33,
    55, 128, 35, 53, 75, 95, 113, 167, 88, 17, 36, 89, 186, 16, 187, 18, 110, 38, 19, 72,
    37, 39, 58, 94, 74, 131, 185, 205, 92, 204, 56, 151, 207, 59, 57, 79, 114, 93, 224, 225,
    150, 168, 226, 206, 112, 115, 169, 170, 78, 132, 99, 227, 171, 76, 96, 77, 189, 191, 228, 133,
    152, 155, 229, 135, 188, 97, 230, 190, 153, 116, 172, 231, 98, 154, 118, 138, 232, 233, 208, 209,
    211, 159, 210, 173, 136, 117, 192, 174, 234, 137, 235, 175, 194, 158, 236, 119, 193, 237, 139, 156,
    238, 157, 176, 239, 215, 240, 195, 213, 214, 198, 241, 212, 178, 179, 177, 196, 242, 197, 243, 199,
    244, 217, 218, 219, 245, 216, 246, 247, 248, 249, 250, 251, 252, 253,
)
JOB_NAMES = (
    ["xn0", "xn1", "xn2", "xn3", "u0", "u1", "v0", "v1", "mix0", "mix1", "mix2", "mix3"]
    + ["out0", "out1", "mid0", "mid1", "mid2", "mid3"]
    + [f"{kind}{j}{i}" for j in range(4) for kind in ("up", "dn") for i in range(2)]
)


def link_bits(fs):
    x, y, z = fs % 4, (fs // 4) % 4, fs // 16
    return {
        "PX": (x + x // 2) % 2,
        "QX": x // 2,
        "PY": (y + y // 2) % 2,
        "QY": y // 2,
        "S": z,
        "O": z,
    }


def place(order, fs):
    bits = link_bits(fs)
    return sum(bits[name] * (1 << k) for k, name in enumerate(order))


def order_of(c, r):
    return CROSSINGS[ORDERS[c][r]]


def gathered_rows(buf, c, first=0, count=SHARDS):
    return jnp.concatenate(
        [
            buf[c, r, place(order_of(c, r), s)]
            for s in range(first, first + count)
            for r in range(PARTS)
        ],
        axis=0,
    )


def rows_of_half(buf, c, half, first, count):
    blocks = []
    for s in range(first, first + count):
        for r in range(PARTS):
            order = order_of(c, r)
            step = max(order.index(z) for z in ("S", "O") if z in order)
            blocks.append(buf[c, r, place(order, s) + half * (1 << step)])
    return jnp.concatenate(blocks, axis=0)


def dot_nt(a, b):
    return lax.dot_general(a, b, (((1,), (1,)), ((), ())), preferred_element_type=F32)


def kernel(
    u_weight,
    v_weight,
    out_weight,
    up_weight,
    down_weight,
    resid,
    mix_matrix,
    out_scale,
    down_scale,
    gain_in,
    gain_out,
    gain_up,
    gain_last,
    u_scale,
    v_scale,
    v_gain,
    mix_bias,
    up_scale,
    result,
    wide,
    buf,
    sbuf,
    scales,
    mix,
    bias,
    xfull,
    nbuf,
    acc,
    vn,
    gated,
    part,
    part_in,
    mid,
    hid,
    terms,
    terms_in,
    stats,
    stats_in,
    load_sem,
    send_sem,
    recv_sem,
    s_send,
    s_recv,
    x_sem,
    pair_send,
    pair_recv,
    out_sem,
):
    rep, fs, lane = lax.axis_index("rep"), lax.axis_index("fs"), lax.axis_index("tp")
    x, y, z = fs % 4, (fs // 4) % 4, fs // 16
    here = z * 16 + y * 4
    far = (1 - z) * 16 + y * 4 + x
    peer = {
        "PX": (rep, here + x + 1 - 2 * (x % 2), lane),
        "QX": (rep, here + 3 - x, lane),
        "PY": (rep, z * 16 + (y + 1 - 2 * (y % 2)) * 4 + x, lane),
        "QY": (rep, z * 16 + (3 - y) * 4 + x, lane),
        "S": (rep, far, lane),
        "O": (1 - rep, far, lane),
    }
    partner = (rep, fs, 1 - lane)
    used = sorted({order_of(c, r) for c in range(NCH) for r in range(PARTS)} | {SCALE_ORDER})
    places = {order: place(order, fs) for order in used}

    barrier = pltpu.get_barrier_semaphore()
    for device in (*peer.values(), partner):
        pl.semaphore_signal(barrier, inc=1, device_id=device, device_id_type=MESH)

    loads = []
    at = 0
    for n, source in enumerate((u_weight, v_weight, out_weight, up_weight, down_weight)):
        span = source.shape[1]
        copy = pltpu.make_async_copy(source, wide.at[:, at : at + span], load_sem.at[n])
        copy.start()
        loads.append(copy)
        at += span
    own_x = pltpu.make_async_copy(resid, xfull.at[lane], x_sem.at[0])
    own_x.start()
    own_mix = pltpu.make_async_copy(mix_matrix, mix, load_sem.at[5])
    own_mix.start()

    def narrow(c, first):
        for r in range(PARTS):
            value = wide[r * TILE : (r + 1) * TILE, first : first + COLS]
            buf[c, r, places[order_of(c, r)]] = value.astype(BF)

    for n in range(3):
        loads[n].wait()
        narrow(n, n * COLS)
    for n in range(2):
        loads[3 + n].wait()
        for j in range(4):
            narrow(3 + 2 * j + n, 3 * COLS + n * WIDTH + j * COLS)
    sbuf[places[SCALE_ORDER], 0:1, 0:64] = out_scale[...]
    sbuf[places[SCALE_ORDER], 1:2, 0:64] = down_scale[...]

    pl.semaphore_wait(barrier, 7)

    other_x = pltpu.make_async_remote_copy(
        src_ref=resid,
        dst_ref=xfull.at[lane],
        send_sem=x_sem.at[1],
        recv_sem=x_sem.at[2],
        device_id=partner,
        device_id_type=MESH,
    )
    other_x.start()

    def send(c, k, r):
        size = 1 << k
        order = order_of(c, r)
        block = buf.at[c, r, pl.ds((places[order] // size) * size, size)]
        pltpu.make_async_remote_copy(
            src_ref=block,
            dst_ref=block,
            send_sem=send_sem.at[c],
            recv_sem=recv_sem.at[c, k, r],
            device_id=peer[order[k]],
            device_id_type=MESH,
        ).start()

    def arrived(c, k, r):
        block = buf.at[c, r, pl.ds(0, 1 << k)]
        pltpu.make_async_copy(block, block, recv_sem.at[c, k, r]).wait()

    complete = set()

    def chunk(c):
        if c not in complete:
            complete.add(c)
            for r in range(PARTS):
                arrived(c, STEPS - 1, r)

    def send_scales(k):
        size = 1 << k
        block = sbuf.at[pl.ds((places[SCALE_ORDER] // size) * size, size)]
        pltpu.make_async_remote_copy(
            src_ref=block,
            dst_ref=block,
            send_sem=s_send.at[k],
            recv_sem=s_recv.at[k],
            device_id=peer[SCALE_ORDER[k]],
            device_id_type=MESH,
        ).start()

    def scales_arrived(k):
        block = sbuf.at[pl.ds(0, 1 << k)]
        pltpu.make_async_copy(block, block, s_recv.at[k]).wait()

    def spread_scales():
        low = lax.broadcasted_iota(jnp.int32, (1, 128), 1) < 64
        for n in range(2):
            for s in range(0, SHARDS, 2):
                a = sbuf[place(SCALE_ORDER, s), n : n + 1, :]
                b = sbuf[place(SCALE_ORDER, s + 1), n : n + 1, :]
                scales[n : n + 1, s * 64 : s * 64 + 128] = jnp.where(low, a, pltpu.roll(b, 64, 1))

    pending, waits, waited = [], {}, set()

    def exchange(src, dst, index, name):
        copy = pltpu.make_async_remote_copy(
            src_ref=src,
            dst_ref=dst,
            send_sem=pair_send.at[index],
            recv_sem=pair_recv.at[index],
            device_id=partner,
            device_id_type=MESH,
        )
        copy.start()
        pending.append(copy)
        waits[name] = copy

    def received(name):
        if name not in waited:
            waited.add(name)
            waits[name].wait_recv()

    def in_rows(first, count, size, body):
        def step(i, carry):
            body(pl.ds(pl.multiple_of(first + i * size, size), size))
            return carry

        lax.fori_loop(0, count // size, step, 0)

    def spread_bias():
        turned = jnp.concatenate([mix_bias[...]] * 16, axis=0).T
        low = lax.broadcasted_iota(jnp.int32, (128, 128), 1) < 64
        for pair in range(4):
            bias[:, pair * 128 : (pair + 1) * 128] = jnp.where(
                low, turned[:, 2 * pair : 2 * pair + 1], turned[:, 2 * pair + 1 : 2 * pair + 2]
            )

    def job_xn(i):
        if i == 0:
            spread_bias()
            own_x.wait()
            other_x.wait()

        def body(rows):
            a = xfull[0, rows, :].astype(F32)
            b = xfull[1, rows, :].astype(F32)
            power = jnp.sum(a * a, axis=1, keepdims=True) + jnp.sum(b * b, axis=1, keepdims=True)
            inv = lax.rsqrt(power / WIDTH + 1e-06)
            nbuf[rows, :HALF] = (a * inv * gain_in[:, :HALF]).astype(BF)
            nbuf[rows, HALF:] = (b * inv * gain_in[:, HALF:]).astype(BF)

        in_rows(i * RB, RB, EB, body)

    def job_u(i):
        chunk(0)
        rows = slice(i * MB, (i + 1) * MB)
        pre = jnp.dot(nbuf[rows, :], gathered_rows(buf, 0), preferred_element_type=F32)
        acc[0, rows, :COLS] = jax.nn.gelu(pre * u_scale[...])

    def job_v(i):
        chunk(1)
        rows = slice(i * MB, (i + 1) * MB)
        pre = jnp.dot(nbuf[rows, :], gathered_rows(buf, 1), preferred_element_type=F32)
        act = jax.nn.gelu(pre * v_scale[...])
        acc[0, rows, COLS:] = act
        total = jnp.sum(act, axis=1, keepdims=True)
        off = act - total / COLS
        spread = jnp.sum(off * off, axis=1, keepdims=True)
        lanes = lax.broadcasted_iota(jnp.int32, (MB, 128), 1)
        stats[0, rows, :] = jnp.where(lanes == 0, total, spread)
        exchange(stats.at[0, pl.ds(i * MB, MB)], stats_in.at[0, pl.ds(i * MB, MB)], i, f"v{i}")

    def job_mix(i):
        received(f"v{i // 2}")
        if i == 0:
            own_mix.wait()

        def body(rows):
            act = acc[0, rows, COLS:]
            own, other = stats[0, rows, :], stats_in[0, rows, :]
            total = own[:, 0:1] + other[:, 0:1]
            apart = (own[:, 0:1] - other[:, 0:1]) / COLS
            spread = own[:, 1:2] + other[:, 1:2] + apart * apart * (COLS / 2)
            centre = total / (2 * COLS)
            inv = lax.rsqrt(spread / (2 * COLS) + 1e-06)
            vn[rows, :] = ((act - centre) * inv * v_gain[...]).astype(BF)

        in_rows(i * RB, RB, 64, body)
        low = lax.broadcasted_iota(jnp.int32, (128, 128), 1) < 64
        for pair in range(4):
            lanes = slice(pair * 128, (pair + 1) * 128)
            m = mix[2 * pair : 2 * pair + 2].astype(BF).reshape(256, 128)
            v = jnp.concatenate(
                [vn[i * RB + b * 128 : i * RB + (b + 1) * 128, lanes] for b in range(2)], axis=1
            )
            both = jnp.dot(m, v, preferred_element_type=F32)
            for b in range(2):
                rows = slice(i * RB + b * 128, i * RB + (b + 1) * 128)
                span = slice(b * 128, (b + 1) * 128)
                mixed = jnp.where(low, both[:128, span], both[128:, span]) + bias[:, lanes]
                gated[rows, lanes] = (acc[0, rows, lanes] * mixed).astype(BF)

    def job_out(i):
        chunk(2)
        rows = slice(i * MB, (i + 1) * MB)
        for q in range(4):
            w = gathered_rows(buf, 2, q * 8, 8)
            part[rows, q * COLS : (q + 1) * COLS] = dot_nt(gated[rows, :], w).astype(BF)
        for n in (2 * i, 2 * i + 1):
            block = pl.ds(n * RB, RB)
            exchange(part.at[block], part_in.at[block], 2 + n, f"out{n}")

    def job_mid(i):
        received(f"out{i}")

        def body(rows):
            total = (part[rows, :].astype(F32) + part_in[rows, :].astype(F32)) * scales[0:1, :]
            inv = lax.rsqrt(jnp.sum(total * total, axis=1, keepdims=True) / WIDTH + 1e-06)
            stream = jnp.concatenate(
                [xfull[0, rows, :].astype(F32), xfull[1, rows, :].astype(F32)], axis=1
            )
            value = (stream + total * inv * gain_out[...]).astype(BF)
            xfull[0, rows, :] = value[:, :HALF]
            xfull[1, rows, :] = value[:, HALF:]
            again = value.astype(F32)
            power = jnp.sum(again * again, axis=1, keepdims=True)
            nbuf[rows, :] = (again * lax.rsqrt(power / WIDTH + 1e-06) * gain_up[...]).astype(BF)

        in_rows(i * RB, RB, EB, body)

    def job_up(j, i):
        c = 3 + 2 * j
        chunk(c)
        rows = slice(i * MB, (i + 1) * MB)
        raised = jnp.dot(nbuf[rows, :], gathered_rows(buf, c), preferred_element_type=F32)
        raised = jnp.maximum(raised * up_scale[:, j * COLS : (j + 1) * COLS], 0.0)
        hid[rows, :] = (raised * raised).astype(BF)

    def job_dn(j, i):
        c = 4 + 2 * j
        chunk(c)
        rows = slice(i * MB, (i + 1) * MB)
        for q in range(4):
            span = slice((q % 2) * COLS, (q % 2 + 1) * COLS)
            term = dot_nt(hid[rows, :], gathered_rows(buf, c, q * 8, 8))
            acc[q // 2, rows, span] = term if j == 0 else acc[q // 2, rows, span] + term

    def last_down(half, i):
        rows = slice(i * MB, (i + 1) * MB)
        for q in range(2):
            span = slice(q * COLS, (q + 1) * COLS)
            term = dot_nt(hid[rows, :], rows_of_half(buf, NCH - 1, half, q * 8, 8))
            yield rows, span, (acc[half, rows, span] + term).astype(BF)

    def job(name):
        kind, index = name.rstrip("0123456789"), [int(n) for n in name[len(name.rstrip("0123456789")) :]]
        {"xn": job_xn, "u": job_u, "v": job_v, "mix": job_mix, "out": job_out, "mid": job_mid, "up": job_up, "dn": job_dn}[kind](*index)

    send_scales(0)
    turns = {50: 1, 90: 2, 120: 3, 150: 4, 165: 5}
    for n, code in enumerate(PROGRAM):
        if n in turns:
            scales_arrived(turns[n] - 1)
            if turns[n] < STEPS:
                send_scales(turns[n])
            else:
                spread_scales()
        if code >= 220:
            name = JOB_NAMES[code - 220]
            if not name.startswith("dn3"):
                job(name)
        else:
            c, k, r = code // 20, (code // 4) % 5, code % 4
            if k:
                arrived(c, k - 1, r)
            send(c, k, r)

    chunk(NCH - 1)
    own, other = lane, 1 - lane
    for i in range(2):
        for rows, span, value in last_down(other, i):
            terms[rows, span] = value
        for n in (2 * i, 2 * i + 1):
            block = pl.ds(n * RB, RB)
            exchange(terms.at[block], terms_in.at[block], 6 + n, f"terms{n}")
    for i in range(2):
        for rows, span, value in last_down(own, i):
            acc[own, rows, span] = value.astype(F32)
    own_cols = pl.ds(pl.multiple_of(lane * HALF, HALF), HALF)

    def add_up(rows):
        value = (acc[own, rows, :] + terms_in[rows, :].astype(F32)) * scales[1:2, own_cols]
        acc[own, rows, :] = value
        power = jnp.sum(value * value, axis=1, keepdims=True)
        stats[1, rows, :] = jnp.broadcast_to(power, (EB, 128))

    def finish(rows):
        power = stats[1, rows, 0:1] + stats_in[1, rows, 0:1]
        inv = lax.rsqrt(power / WIDTH + 1e-06)
        value = acc[own, rows, :] * inv * gain_last[:, own_cols]
        mid[rows, :] = (xfull[lane, rows, :].astype(F32) + value).astype(BF)

    for i in range(NRB):
        received(f"terms{i}")
        in_rows(i * RB, RB, EB, add_up)
        block = pl.ds(i * RB, RB)
        exchange(stats.at[1, block], stats_in.at[1, block], 10 + i, f"power{i}")
    outs = []
    for i in range(NRB):
        received(f"power{i}")
        in_rows(i * RB, RB, EB, finish)
        block = pl.ds(i * RB, RB)
        copy = pltpu.make_async_copy(mid.at[block], result.at[block], out_sem.at[i])
        copy.start()
        outs.append(copy)
    for copy in outs:
        copy.wait()
    for copy in pending:
        copy.wait_send()
    for c in range(NCH):
        block = buf.at[c, :, pl.ds(0, 31)]
        pltpu.make_async_copy(block, block, send_sem.at[c]).wait()
    for k in range(STEPS):
        block = sbuf.at[pl.ds(0, 1 << k)]
        pltpu.make_async_copy(block, block, s_send.at[k]).wait()


def local(
    resid,
    gain_mix_in,
    u_weight,
    v_weight,
    u_scale,
    v_scale,
    v_gain,
    mix_matrix,
    mix_bias,
    out_weight,
    out_scale,
    gain_mix_out,
    gain_ffn_in,
    up_weight,
    up_scale,
    down_weight,
    down_scale,
    gain_ffn_out,
):
    row = lambda a: a.reshape(1, -1)
    vmem = pl.BlockSpec(memory_space=pltpu.VMEM)
    hbm = pl.BlockSpec(memory_space=pl.ANY)
    dma = pltpu.SemaphoreType.DMA
    return pl.pallas_call(
        kernel,
        out_shape=jax.ShapeDtypeStruct((ROWS, HALF), BF),
        in_specs=[hbm] * 7 + [vmem] * 11,
        out_specs=hbm,
        scratch_shapes=[
            pltpu.VMEM((64, 3 * COLS + 2 * WIDTH), F32),
            pltpu.VMEM((NCH, PARTS, SHARDS, TILE, COLS), BF),
            pltpu.VMEM((SHARDS, 2, 128), F32),
            pltpu.VMEM((2, WIDTH), F32),
            pltpu.VMEM((8, 128, 128), F32),
            pltpu.VMEM((128, COLS), F32),
            pltpu.VMEM((2, ROWS, HALF), BF),
            pltpu.VMEM((ROWS, WIDTH), BF),
            pltpu.VMEM((2, ROWS, HALF), F32),
            pltpu.VMEM((ROWS, COLS), BF),
            pltpu.VMEM((ROWS, COLS), BF),
            pltpu.VMEM((ROWS, WIDTH), BF),
            pltpu.VMEM((ROWS, WIDTH), BF),
            pltpu.VMEM((ROWS, HALF), BF),
            pltpu.VMEM((ROWS, COLS), BF),
            pltpu.VMEM((ROWS, HALF), BF),
            pltpu.VMEM((ROWS, HALF), BF),
            pltpu.VMEM((2, ROWS, 128), F32),
            pltpu.VMEM((2, ROWS, 128), F32),
            dma((6,)),
            dma((NCH,)),
            dma((NCH, STEPS, PARTS)),
            dma((STEPS,)),
            dma((STEPS,)),
            dma((3,)),
            dma((14,)),
            dma((14,)),
            dma((NRB,)),
        ],
        compiler_params=pltpu.CompilerParams(
            collective_id=0, has_side_effects=True, vmem_limit_bytes=67043328
        ),
    )(
        u_weight,
        v_weight,
        out_weight.T,
        up_weight,
        down_weight.T,
        resid,
        mix_matrix,
        row(out_scale),
        row(down_scale),
        row(gain_mix_in),
        row(gain_mix_out),
        row(gain_ffn_in),
        row(gain_ffn_out),
        row(u_scale),
        row(v_scale),
        row(v_gain),
        mix_bias,
        row(up_scale),
    )


def solution(mesh):
    in_specs = (
        P(("rep", "fs"), "tp"),
        P(),
        P("fs", "tp"),
        P("fs", "tp"),
        P("tp"),
        P("tp"),
        P("tp"),
        P("tp", None, None),
        P("tp", None),
        P("tp", "fs"),
        P("fs"),
        P(),
        P(),
        P("fs", "tp"),
        P("tp"),
        P("tp", "fs"),
        P("fs"),
        P(),
    )
    out_specs = P(("rep", "fs"), "tp")
    return jax.shard_map(local, mesh=mesh, in_specs=in_specs, out_specs=out_specs, check_vma=False)
```

time: 143 us -> 109 us (0.76)
  Pallas kernels: 132 us -> 105 us
  other arithmetic: 6.21 us -> 0 us
  local copies, waits for them, and re-layouts: 4.7 us -> 3.08 us
    pallas_call x1, Pallas kernels: 132 us -> 105 us  [local(): pl.pallas_call(kernel, out_shape=jax.ShapeDtypeStruct((ROWS, HALF), BF),...]
    another operation x6 -> x0, other arithmetic: 3.9 us -> none
    unnamed x3 -> x1, local copies, waits for them, and re-layouts: 3.08 us -> 3.08 us
where the time goes in v2:
time: 109 us; the launch traced here: 108 us
  Pallas kernels  105 us (96%)
  local copies, waits for them, and re-layouts  3.08 us (3%)
    pallas_call x1, Pallas kernels, local(): pl.pallas_call(kernel, out_shape=jax.ShapeDtypeStruct((ROWS, HALF), BF),...  105 us
    unnamed x1, local copies, waits for them, and re-layouts  3.08 us

profile of v2, /device:TPU:1, one launch (start us, length us, event | category | flops | bytes accessed | tf_op | source)
XLA Modules:
  0.0 108.5 jit_solution(6861950010291731848)
XLA Ops:
  0.0 105.4 %shard_map.172 = bf16[1024,1024]{1,0:T(8,128)(2,1)} custom-call(f32[64,512]{1,0:T(8,128)} %u_weight.1, f32[64,512]{1,0:T(8,128)} %v_weight.1, f32[64,512]{1,0:T(8,128)} %bitcast.13, f32[64,2048]{1,0:T(8,128)} %up_weight.1, f32[64,2048]{1,0:T(8,128)} %bitcast.12, bf16[1024,1024]{1,0:T(8,128)(2,1)} %resid.1, f32[8,128,128]{2,1,0:T(8,128)} %mix_matrix.1, ...), custom_call_target="tpu_custom_call" | custom-call | tf_op jit(solution)/shard_map/pallas_call | solution.py:522
  105.4 3.1 %copy.20 = bf16[1024,1024]{1,0:T(8,128)(2,1)} copy(bf16[1024,1024]{1,0:T(8,128)(2,1)} %shard_map.172) | data formatting | bytes 4194304

commit v3 on v2

--- a/solution.py
+++ b/solution.py
@@ -24,6 +24,8 @@
 NRB = ROWS // RB
 MB = 512
 EB = 32
+AT_ONCE = 2
+VMEM_LIMIT = 56 * 1024 * 1024
 
 CROSSINGS = [
     order
@@ -31,33 +33,33 @@
     for order in itertools.permutations(("PX", "QX", "PY", "QY", z))
 ]
 ORDERS = (
-    (24, 123, 198, 39),
-    (88, 195, 178, 80),
-    (49, 95, 150, 78),
-    (197, 183, 132, 126),
-    (78, 36, 111, 7),
-    (182, 153, 108, 63),
-    (12, 129, 27, 66),
-    (5, 173, 194, 192),
-    (12, 142, 48, 111),
-    (42, 75, 156, 158),
-    (76, 12, 35, 169),
+    (58, 77, 30, 176),
+    (126, 202, 51, 8),
+    (63, 127, 5, 84),
+    (146, 81, 206, 24),
+    (80, 177, 161, 137),
+    (194, 170, 6, 210),
+    (172, 26, 194, 177),
+    (72, 139, 62, 143),
+    (5, 120, 41, 44),
+    (185, 24, 126, 195),
+    (47, 98, 5, 129),
 )
 SCALE_ORDER = ("PX", "QY", "QX", "PY", "S")
 PROGRAM = (
-    0, 1, 2, 3, 20, 21, 22, 23, 40, 41, 42, 43, 61, 62, 63, 81, 82, 83, 100, 101,
-    102, 103, 120, 60, 121, 122, 123, 140, 141, 163, 180, 182, 160, 80, 162, 183, 161, 142, 203, 202,
-    201, 143, 181, 200, 4, 5, 6, 26, 7, 66, 24, 86, 44, 46, 25, 65, 67, 27, 45, 85,
-    87, 126, 47, 127, 184, 64, 144, 104, 145, 105, 165, 84, 146, 107, 106, 147, 124, 125, 28, 166,
-    9, 8, 48, 220, 10, 30, 70, 164, 221, 11, 50, 68, 69, 130, 222, 29, 51, 71, 109, 148,
-    149, 223, 31, 32, 90, 52, 129, 49, 13, 91, 12, 14, 15, 108, 34, 73, 111, 54, 134, 33,
-    55, 128, 35, 53, 75, 95, 113, 167, 88, 17, 36, 89, 186, 16, 187, 18, 110, 38, 19, 72,
-    37, 39, 58, 94, 74, 131, 185, 205, 92, 204, 56, 151, 207, 59, 57, 79, 114, 93, 224, 225,
-    150, 168, 226, 206, 112, 115, 169, 170, 78, 132, 99, 227, 171, 76, 96, 77, 189, 191, 228, 133,
-    152, 155, 229, 135, 188, 97, 230, 190, 153, 116, 172, 231, 98, 154, 118, 138, 232, 233, 208, 209,
-    211, 159, 210, 173, 136, 117, 192, 174, 234, 137, 235, 175, 194, 158, 236, 119, 193, 237, 139, 156,
-    238, 157, 176, 239, 215, 240, 195, 213, 214, 198, 241, 212, 178, 179, 177, 196, 242, 197, 243, 199,
-    244, 217, 218, 219, 245, 216, 246, 247, 248, 249, 250, 251, 252, 253,
+    0, 1, 2, 3, 20, 21, 22, 23, 40, 41, 42, 43, 60, 61, 62, 63, 80, 81, 82, 83,
+    100, 101, 102, 103, 120, 121, 123, 141, 142, 122, 143, 162, 160, 163, 181, 200, 180, 140, 201, 161,
+    183, 182, 202, 203, 4, 6, 5, 24, 7, 25, 27, 26, 45, 44, 65, 86, 46, 64, 87, 47,
+    166, 84, 67, 145, 167, 66, 107, 147, 146, 85, 104, 204, 106, 184, 220, 8, 10, 11, 48, 186,
+    221, 9, 28, 29, 31, 105, 69, 124, 90, 222, 30, 49, 50, 51, 71, 91, 170, 223, 12, 68,
+    70, 88, 188, 108, 89, 127, 52, 110, 13, 14, 15, 128, 73, 35, 53, 94, 32, 33, 34, 55,
+    93, 72, 16, 125, 164, 126, 18, 17, 144, 19, 111, 95, 74, 37, 54, 36, 39, 92, 165, 38,
+    109, 185, 75, 187, 56, 130, 224, 129, 58, 59, 76, 225, 131, 148, 149, 57, 150, 205, 77, 78,
+    79, 112, 226, 207, 169, 227, 151, 113, 171, 133, 228, 114, 115, 168, 135, 97, 229, 96, 189, 153,
+    230, 206, 132, 191, 152, 116, 231, 98, 208, 232, 134, 155, 118, 211, 233, 117, 172, 99, 119, 173,
+    154, 234, 210, 136, 235, 175, 190, 137, 138, 236, 209, 139, 192, 174, 237, 238, 193, 159, 157, 239,
+    195, 156, 240, 194, 241, 215, 178, 242, 212, 213, 214, 158, 177, 243, 244, 176, 179, 196, 199, 245,
+    198, 197, 217, 219, 216, 218, 246, 247, 248, 249, 250, 251, 252, 253,
 )
 JOB_NAMES = (
     ["xn0", "xn1", "xn2", "xn3", "u0", "u1", "v0", "v1", "mix0", "mix1", "mix2", "mix3"]
@@ -132,7 +134,6 @@
     mix_bias,
     up_scale,
     result,
-    wide,
     buf,
     sbuf,
     scales,
@@ -145,9 +146,6 @@
     gated,
     part,
     part_in,
-    mid,
-    hid,
-    terms,
     terms_in,
     stats,
     stats_in,
@@ -159,7 +157,6 @@
     x_sem,
     pair_send,
     pair_recv,
-    out_sem,
 ):
     rep, fs, lane = lax.axis_index("rep"), lax.axis_index("fs"), lax.axis_index("tp")
     x, y, z = fs % 4, (fs // 4) % 4, fs // 16
@@ -182,30 +179,28 @@
         pl.semaphore_signal(barrier, inc=1, device_id=device, device_id_type=MESH)
 
     loads = []
-    at = 0
-    for n, source in enumerate((u_weight, v_weight, out_weight, up_weight, down_weight)):
-        span = source.shape[1]
-        copy = pltpu.make_async_copy(source, wide.at[:, at : at + span], load_sem.at[n])
+
+    def load(source, first, c, sem):
+        slot = acc.at[0, pl.ds(c * 64, 64), pl.ds(0, COLS)]
+        copy = pltpu.make_async_copy(source.at[:, pl.ds(first, COLS)], slot, load_sem.at[sem])
         copy.start()
         loads.append(copy)
-        at += span
+
+    for n, source in enumerate((u_weight, v_weight, out_weight)):
+        load(source, 0, n, n)
+    for j in range(4):
+        load(up_weight, j * COLS, 3 + 2 * j, 3 + 2 * j)
+        load(down_weight, j * COLS, 4 + 2 * j, 4 + 2 * j)
     own_x = pltpu.make_async_copy(resid, xfull.at[lane], x_sem.at[0])
     own_x.start()
-    own_mix = pltpu.make_async_copy(mix_matrix, mix, load_sem.at[5])
+    own_mix = pltpu.make_async_copy(mix_matrix, mix, load_sem.at[NCH])
     own_mix.start()
 
-    def narrow(c, first):
+    for c in range(NCH):
+        loads[c].wait()
         for r in range(PARTS):
-            value = wide[r * TILE : (r + 1) * TILE, first : first + COLS]
+            value = acc[0, c * 64 + r * TILE : c * 64 + (r + 1) * TILE, :COLS]
             buf[c, r, places[order_of(c, r)]] = value.astype(BF)
-
-    for n in range(3):
-        loads[n].wait()
-        narrow(n, n * COLS)
-    for n in range(2):
-        loads[3 + n].wait()
-        for j in range(4):
-            narrow(3 + 2 * j + n, 3 * COLS + n * WIDTH + j * COLS)
     sbuf[places[SCALE_ORDER], 0:1, 0:64] = out_scale[...]
     sbuf[places[SCALE_ORDER], 1:2, 0:64] = down_scale[...]
 
@@ -270,7 +265,7 @@
                 b = sbuf[place(SCALE_ORDER, s + 1), n : n + 1, :]
                 scales[n : n + 1, s * 64 : s * 64 + 128] = jnp.where(low, a, pltpu.roll(b, 64, 1))
 
-    pending, waits, waited = [], {}, set()
+    pending, waits, waited = {}, {}, set()
 
     def exchange(src, dst, index, name):
         copy = pltpu.make_async_remote_copy(
@@ -282,7 +277,7 @@
             device_id_type=MESH,
         )
         copy.start()
-        pending.append(copy)
+        pending[name] = copy
         waits[name] = copy
 
     def received(name):
@@ -290,12 +285,16 @@
             waited.add(name)
             waits[name].wait_recv()
 
-    def in_rows(first, count, size, body):
+    def sent(name):
+        pending.pop(name).wait_send()
+
+    def in_rows(first, count, size, body, at_once=1):
         def step(i, carry):
-            body(pl.ds(pl.multiple_of(first + i * size, size), size))
+            for n in range(at_once):
+                body(pl.ds(pl.multiple_of(first + (i * at_once + n) * size, size), size))
             return carry
 
-        lax.fori_loop(0, count // size, step, 0)
+        lax.fori_loop(0, count // (size * at_once), step, 0)
 
     def spread_bias():
         turned = jnp.concatenate([mix_bias[...]] * 16, axis=0).T
@@ -319,7 +318,7 @@
             nbuf[rows, :HALF] = (a * inv * gain_in[:, :HALF]).astype(BF)
             nbuf[rows, HALF:] = (b * inv * gain_in[:, HALF:]).astype(BF)
 
-        in_rows(i * RB, RB, EB, body)
+        in_rows(i * RB, RB, EB, body, AT_ONCE)
 
     def job_u(i):
         chunk(0)
@@ -396,7 +395,7 @@
             power = jnp.sum(again * again, axis=1, keepdims=True)
             nbuf[rows, :] = (again * lax.rsqrt(power / WIDTH + 1e-06) * gain_up[...]).astype(BF)
 
-        in_rows(i * RB, RB, EB, body)
+        in_rows(i * RB, RB, EB, body, AT_ONCE)
 
     def job_up(j, i):
         c = 3 + 2 * j
@@ -404,7 +403,7 @@
         rows = slice(i * MB, (i + 1) * MB)
         raised = jnp.dot(nbuf[rows, :], gathered_rows(buf, c), preferred_element_type=F32)
         raised = jnp.maximum(raised * up_scale[:, j * COLS : (j + 1) * COLS], 0.0)
-        hid[rows, :] = (raised * raised).astype(BF)
+        vn[rows, :] = (raised * raised).astype(BF)
 
     def job_dn(j, i):
         c = 4 + 2 * j
@@ -412,14 +411,14 @@
         rows = slice(i * MB, (i + 1) * MB)
         for q in range(4):
             span = slice((q % 2) * COLS, (q % 2 + 1) * COLS)
-            term = dot_nt(hid[rows, :], gathered_rows(buf, c, q * 8, 8))
+            term = dot_nt(vn[rows, :], gathered_rows(buf, c, q * 8, 8))
             acc[q // 2, rows, span] = term if j == 0 else acc[q // 2, rows, span] + term
 
     def last_down(half, i):
         rows = slice(i * MB, (i + 1) * MB)
         for q in range(2):
             span = slice(q * COLS, (q + 1) * COLS)
-            term = dot_nt(hid[rows, :], rows_of_half(buf, NCH - 1, half, q * 8, 8))
+            term = dot_nt(vn[rows, :], rows_of_half(buf, NCH - 1, half, q * 8, 8))
             yield rows, span, (acc[half, rows, span] + term).astype(BF)
 
     def job(name):
@@ -445,14 +444,16 @@
                 arrived(c, k - 1, r)
             send(c, k, r)
 
+    for i in range(NRB):
+        sent(f"out{i}")
     chunk(NCH - 1)
     own, other = lane, 1 - lane
     for i in range(2):
         for rows, span, value in last_down(other, i):
-            terms[rows, span] = value
+            part[rows, span] = value
         for n in (2 * i, 2 * i + 1):
             block = pl.ds(n * RB, RB)
-            exchange(terms.at[block], terms_in.at[block], 6 + n, f"terms{n}")
+            exchange(part.at[block, pl.ds(0, HALF)], terms_in.at[block], 6 + n, f"terms{n}")
     for i in range(2):
         for rows, span, value in last_down(own, i):
             acc[own, rows, span] = value.astype(F32)
@@ -468,24 +469,17 @@
         power = stats[1, rows, 0:1] + stats_in[1, rows, 0:1]
         inv = lax.rsqrt(power / WIDTH + 1e-06)
         value = acc[own, rows, :] * inv * gain_last[:, own_cols]
-        mid[rows, :] = (xfull[lane, rows, :].astype(F32) + value).astype(BF)
+        result[rows, :] = (xfull[lane, rows, :].astype(F32) + value).astype(BF)
 
     for i in range(NRB):
         received(f"terms{i}")
-        in_rows(i * RB, RB, EB, add_up)
+        in_rows(i * RB, RB, EB, add_up, AT_ONCE)
         block = pl.ds(i * RB, RB)
         exchange(stats.at[1, block], stats_in.at[1, block], 10 + i, f"power{i}")
-    outs = []
     for i in range(NRB):
         received(f"power{i}")
-        in_rows(i * RB, RB, EB, finish)
-        block = pl.ds(i * RB, RB)
-        copy = pltpu.make_async_copy(mid.at[block], result.at[block], out_sem.at[i])
-        copy.start()
-        outs.append(copy)
-    for copy in outs:
-        copy.wait()
-    for copy in pending:
+        in_rows(i * RB, RB, EB, finish, AT_ONCE)
+    for copy in pending.values():
         copy.wait_send()
     for c in range(NCH):
         block = buf.at[c, :, pl.ds(0, 31)]
@@ -521,11 +515,10 @@
     dma = pltpu.SemaphoreType.DMA
     return pl.pallas_call(
         kernel,
-        out_shape=jax.ShapeDtypeStruct((ROWS, HALF), BF),
+        out_shape=pltpu.VMEM((ROWS, HALF), BF),
         in_specs=[hbm] * 7 + [vmem] * 11,
-        out_specs=hbm,
+        out_specs=vmem,
         scratch_shapes=[
-            pltpu.VMEM((64, 3 * COLS + 2 * WIDTH), F32),
             pltpu.VMEM((NCH, PARTS, SHARDS, TILE, COLS), BF),
             pltpu.VMEM((SHARDS, 2, 128), F32),
             pltpu.VMEM((2, WIDTH), F32),
@@ -539,12 +532,9 @@
             pltpu.VMEM((ROWS, WIDTH), BF),
             pltpu.VMEM((ROWS, WIDTH), BF),
             pltpu.VMEM((ROWS, HALF), BF),
-            pltpu.VMEM((ROWS, COLS), BF),
-            pltpu.VMEM((ROWS, HALF), BF),
-            pltpu.VMEM((ROWS, HALF), BF),
             pltpu.VMEM((2, ROWS, 128), F32),
             pltpu.VMEM((2, ROWS, 128), F32),
-            dma((6,)),
+            dma((NCH + 1,)),
             dma((NCH,)),
             dma((NCH, STEPS, PARTS)),
             dma((STEPS,)),
@@ -552,10 +542,9 @@
             dma((3,)),
             dma((14,)),
             dma((14,)),
-            dma((NRB,)),
         ],
         compiler_params=pltpu.CompilerParams(
-            collective_id=0, has_side_effects=True, vmem_limit_bytes=67043328
+            collective_id=0, has_side_effects=True, vmem_limit_bytes=VMEM_LIMIT
         ),
     )(
         u_weight,

time: 109 us -> 104 us (0.954)
  Pallas kernels: 105 us -> 103 us
  local copies, waits for them, and re-layouts: 3.08 us -> 1.32 us
    pallas_call x1, Pallas kernels: 105 us -> 103 us  [local(): pl.pallas_call(kernel, out_shape=pltpu.VMEM((ROWS, HALF), BF), in_specs=[...]
    unnamed x1, local copies, waits for them, and re-layouts: 3.08 us -> 1.32 us
where the time goes in v3:
time: 104 us
  Pallas kernels  103 us (99%)
  local copies, waits for them, and re-layouts  1.32 us (1%)
    pallas_call x1, Pallas kernels, local(): pl.pallas_call(kernel, out_shape=pltpu.VMEM((ROWS, HALF), BF), in_specs=[...  103 us

profile of v3, /device:TPU:1, one launch (start us, length us, event | category | flops | bytes accessed | tf_op | source)
XLA Modules:
  0.0 104.0 jit_solution(7751198018864355697)
XLA Ops:
  0.0 102.6 %shard_map.172 = bf16[1024,1024]{1,0:T(8,128)(2,1)S(1)} custom-call(f32[64,512]{1,0:T(8,128)} %u_weight.1, f32[64,512]{1,0:T(8,128)} %v_weight.1, f32[64,512]{1,0:T(8,128)} %bitcast.13, f32[64,2048]{1,0:T(8,128)} %up_weight.1, f32[64,2048]{1,0:T(8,128)} %bitcast.12, bf16[1024,1024]{1,0:T(8,128)(2,1)} %resid.1, f32[8,128,128]{2,1,0:T(8,128)} %mix_matrix.1, ...), custom_call_target="tpu_custom_call" | custom-call | tf_op jit(solution)/shard_map/pallas_call | solution.py:516
  102.6 1.3 %copy.20 = bf16[1024,1024]{1,0:T(8,128)(2,1)} copy(bf16[1024,1024]{1,0:T(8,128)(2,1)S(1)} %shard_map.172) | data formatting | bytes 4194304

commit v4 on v3

--- a/solution.py
+++ b/solution.py
@@ -16,6 +16,7 @@
 HALF = 1024
 COLS = 512
 NCH = 11
+LAST = NCH - 1
 STEPS = 5
 SHARDS = 32
 TILE = 16
@@ -25,7 +26,7 @@
 MB = 512
 EB = 32
 AT_ONCE = 2
-VMEM_LIMIT = 56 * 1024 * 1024
+VMEM_LIMIT = 58 * 1024 * 1024
 
 CROSSINGS = [
     order
@@ -33,38 +34,39 @@
     for order in itertools.permutations(("PX", "QX", "PY", "QY", z))
 ]
 ORDERS = (
-    (58, 77, 30, 176),
-    (126, 202, 51, 8),
-    (63, 127, 5, 84),
-    (146, 81, 206, 24),
-    (80, 177, 161, 137),
-    (194, 170, 6, 210),
-    (172, 26, 194, 177),
-    (72, 139, 62, 143),
-    (5, 120, 41, 44),
-    (185, 24, 126, 195),
-    (47, 98, 5, 129),
+    (193, 13, 158, 48),
+    (146, 153, 88, 60),
+    (6, 180, 124, 209),
+    (72, 145, 9, 186),
+    (144, 82, 24, 128),
+    (87, 156, 64, 72),
+    (38, 230, 125, 180),
+    (5, 201, 38, 122),
+    (24, 191, 128, 188),
+    (92, 64, 168, 8),
+    (119, 114, 96, 99),
 )
 SCALE_ORDER = ("PX", "QY", "QX", "PY", "S")
 PROGRAM = (
     0, 1, 2, 3, 20, 21, 22, 23, 40, 41, 42, 43, 60, 61, 62, 63, 80, 81, 82, 83,
-    100, 101, 102, 103, 120, 121, 123, 141, 142, 122, 143, 162, 160, 163, 181, 200, 180, 140, 201, 161,
-    183, 182, 202, 203, 4, 6, 5, 24, 7, 25, 27, 26, 45, 44, 65, 86, 46, 64, 87, 47,
-    166, 84, 67, 145, 167, 66, 107, 147, 146, 85, 104, 204, 106, 184, 220, 8, 10, 11, 48, 186,
-    221, 9, 28, 29, 31, 105, 69, 124, 90, 222, 30, 49, 50, 51, 71, 91, 170, 223, 12, 68,
-    70, 88, 188, 108, 89, 127, 52, 110, 13, 14, 15, 128, 73, 35, 53, 94, 32, 33, 34, 55,
-    93, 72, 16, 125, 164, 126, 18, 17, 144, 19, 111, 95, 74, 37, 54, 36, 39, 92, 165, 38,
-    109, 185, 75, 187, 56, 130, 224, 129, 58, 59, 76, 225, 131, 148, 149, 57, 150, 205, 77, 78,
-    79, 112, 226, 207, 169, 227, 151, 113, 171, 133, 228, 114, 115, 168, 135, 97, 229, 96, 189, 153,
-    230, 206, 132, 191, 152, 116, 231, 98, 208, 232, 134, 155, 118, 211, 233, 117, 172, 99, 119, 173,
-    154, 234, 210, 136, 235, 175, 190, 137, 138, 236, 209, 139, 192, 174, 237, 238, 193, 159, 157, 239,
-    195, 156, 240, 194, 241, 215, 178, 242, 212, 213, 214, 158, 177, 243, 244, 176, 179, 196, 199, 245,
-    198, 197, 217, 219, 216, 218, 246, 247, 248, 249, 250, 251, 252, 253,
+    100, 101, 102, 103, 121, 122, 123, 140, 141, 120, 143, 161, 163, 200, 201, 202, 180, 162, 142, 181,
+    203, 183, 160, 182, 4, 5, 6, 7, 26, 44, 27, 24, 46, 25, 45, 67, 64, 85, 47, 106,
+    126, 65, 144, 66, 165, 105, 145, 167, 84, 184, 87, 147, 124, 220, 8, 30, 86, 50, 10, 107,
+    127, 221, 9, 31, 28, 104, 89, 130, 222, 11, 29, 49, 51, 125, 110, 166, 223, 69, 70, 148,
+    71, 48, 88, 91, 12, 14, 68, 32, 146, 13, 35, 185, 33, 151, 34, 74, 90, 15, 73, 53,
+    54, 109, 189, 52, 18, 164, 55, 131, 16, 39, 37, 92, 108, 111, 94, 19, 36, 75, 17, 93,
+    58, 38, 59, 56, 57, 72, 77, 129, 128, 95, 224, 186, 187, 149, 112, 114, 96, 225, 150, 76,
+    78, 79, 206, 226, 113, 227, 207, 228, 132, 229, 115, 99, 230, 231, 204, 171, 133, 98, 232, 205,
+    168, 135, 233, 234, 169, 97, 154, 170, 235, 188, 153, 236, 134, 237, 190, 116, 117, 119, 238, 118,
+    239, 191, 155, 240, 152, 241, 208, 209, 242, 210, 211, 172, 175, 136, 139, 243, 173, 138, 244, 137,
+    192, 245, 174, 246, 193, 158, 159, 247, 195, 156, 194, 157, 212, 215, 176, 178, 248, 213, 214, 249,
+    177, 179, 197, 196, 198, 199, 250, 251, 216, 218, 219, 217, 252, 253, 254, 255, 256, 257,
 )
 JOB_NAMES = (
-    ["xn0", "xn1", "xn2", "xn3", "u0", "u1", "v0", "v1", "mix0", "mix1", "mix2", "mix3"]
-    + ["out0", "out1", "mid0", "mid1", "mid2", "mid3"]
-    + [f"{kind}{j}{i}" for j in range(4) for kind in ("up", "dn") for i in range(2)]
+    ["xn0", "xn1", "xn2", "xn3", "v0", "v1", "vn0", "vn1", "u0", "mix0", "mix1", "out0"]
+    + ["vn2", "vn3", "u1", "mix2", "mix3", "out1", "mid0", "mid1", "up00", "mid2", "mid3", "up01"]
+    + ["dn00", "dn01"]
+    + [f"{kind}{j}{i}" for j in range(1, 4) for kind in ("up", "dn") for i in range(2)]
 )
 
 
@@ -98,16 +100,6 @@
         ],
         axis=0,
     )
-
-
-def rows_of_half(buf, c, half, first, count):
-    blocks = []
-    for s in range(first, first + count):
-        for r in range(PARTS):
-            order = order_of(c, r)
-            step = max(order.index(z) for z in ("S", "O") if z in order)
-            blocks.append(buf[c, r, place(order, s) + half * (1 << step)])
-    return jnp.concatenate(blocks, axis=0)
 
 
 def dot_nt(a, b):
@@ -143,6 +135,8 @@
     nbuf,
     acc,
     vn,
+    both_hid,
+    stage,
     gated,
     part,
     part_in,
@@ -152,6 +146,8 @@
     load_sem,
     send_sem,
     recv_sem,
+    first_send,
+    first_recv,
     s_send,
     s_recv,
     x_sem,
@@ -171,11 +167,13 @@
         "O": (1 - rep, far, lane),
     }
     partner = (rep, fs, 1 - lane)
+    across = (rep, far, 1 - lane)
+    crossed = lane + z - 2 * lane * z
     used = sorted({order_of(c, r) for c in range(NCH) for r in range(PARTS)} | {SCALE_ORDER})
     places = {order: place(order, fs) for order in used}
 
     barrier = pltpu.get_barrier_semaphore()
-    for device in (*peer.values(), partner):
+    for device in (*peer.values(), partner, across):
         pl.semaphore_signal(barrier, inc=1, device_id=device, device_id_type=MESH)
 
     loads = []
@@ -186,7 +184,7 @@
         copy.start()
         loads.append(copy)
 
-    for n, source in enumerate((u_weight, v_weight, out_weight)):
+    for n, source in enumerate((v_weight, u_weight, out_weight)):
         load(source, 0, n, n)
     for j in range(4):
         load(up_weight, j * COLS, 3 + 2 * j, 3 + 2 * j)
@@ -200,11 +198,23 @@
         loads[c].wait()
         for r in range(PARTS):
             value = acc[0, c * 64 + r * TILE : c * 64 + (r + 1) * TILE, :COLS]
-            buf[c, r, places[order_of(c, r)]] = value.astype(BF)
+            if c < LAST:
+                buf[c, r, places[order_of(c, r)]] = value.astype(BF)
+            else:
+                stage[r] = value.astype(BF)
+
+    def last_slot(r):
+        return place(order_of(LAST, r), lane * 16 + y * 4 + x)
+
+    @pl.when(crossed == 0)
+    def _():
+        for r in range(PARTS):
+            buf[LAST, r, last_slot(r)] = stage[r]
+
     sbuf[places[SCALE_ORDER], 0:1, 0:64] = out_scale[...]
     sbuf[places[SCALE_ORDER], 1:2, 0:64] = down_scale[...]
 
-    pl.semaphore_wait(barrier, 7)
+    pl.semaphore_wait(barrier, 8)
 
     other_x = pltpu.make_async_remote_copy(
         src_ref=resid,
@@ -215,6 +225,38 @@
         device_id_type=MESH,
     )
     other_x.start()
+
+    def first_of_last(r):
+        slot = buf.at[LAST, r, last_slot(r)]
+        pltpu.make_async_remote_copy(
+            src_ref=stage.at[r],
+            dst_ref=slot,
+            send_sem=send_sem.at[LAST],
+            recv_sem=first_recv.at[crossed, r],
+            device_id=(rep, far, z),
+            device_id_type=MESH,
+        ).start()
+
+        @pl.when(crossed == 1)
+        def _():
+            pltpu.make_async_remote_copy(
+                src_ref=stage.at[r],
+                dst_ref=slot,
+                send_sem=first_send.at[r],
+                recv_sem=first_recv.at[2, r],
+                device_id=partner,
+                device_id_type=MESH,
+            ).start()
+
+    def first_of_last_arrived(r):
+        @pl.when(crossed == 1)
+        def _():
+            for n in range(2):
+                pltpu.make_async_copy(stage.at[r], stage.at[r], first_recv.at[n, r]).wait()
+
+        @pl.when(crossed == 0)
+        def _():
+            pltpu.make_async_copy(stage.at[r], stage.at[r], first_recv.at[2, r]).wait()
 
     def send(c, k, r):
         size = 1 << k
@@ -321,15 +363,15 @@
         in_rows(i * RB, RB, EB, body, AT_ONCE)
 
     def job_u(i):
+        chunk(1)
+        rows = slice(i * MB, (i + 1) * MB)
+        pre = jnp.dot(nbuf[rows, :], gathered_rows(buf, 1), preferred_element_type=F32)
+        acc[0, rows, :COLS] = jax.nn.gelu(pre * u_scale[...])
+
+    def job_v(i):
         chunk(0)
         rows = slice(i * MB, (i + 1) * MB)
         pre = jnp.dot(nbuf[rows, :], gathered_rows(buf, 0), preferred_element_type=F32)
-        acc[0, rows, :COLS] = jax.nn.gelu(pre * u_scale[...])
-
-    def job_v(i):
-        chunk(1)
-        rows = slice(i * MB, (i + 1) * MB)
-        pre = jnp.dot(nbuf[rows, :], gathered_rows(buf, 1), preferred_element_type=F32)
         act = jax.nn.gelu(pre * v_scale[...])
         acc[0, rows, COLS:] = act
         total = jnp.sum(act, axis=1, keepdims=True)
@@ -339,10 +381,8 @@
         stats[0, rows, :] = jnp.where(lanes == 0, total, spread)
         exchange(stats.at[0, pl.ds(i * MB, MB)], stats_in.at[0, pl.ds(i * MB, MB)], i, f"v{i}")
 
-    def job_mix(i):
+    def job_vn(i):
         received(f"v{i // 2}")
-        if i == 0:
-            own_mix.wait()
 
         def body(rows):
             act = acc[0, rows, COLS:]
@@ -355,6 +395,10 @@
             vn[rows, :] = ((act - centre) * inv * v_gain[...]).astype(BF)
 
         in_rows(i * RB, RB, 64, body)
+
+    def job_mix(i):
+        if i == 0:
+            own_mix.wait()
         low = lax.broadcasted_iota(jnp.int32, (128, 128), 1) < 64
         for pair in range(4):
             lanes = slice(pair * 128, (pair + 1) * 128)
@@ -403,7 +447,12 @@
         rows = slice(i * MB, (i + 1) * MB)
         raised = jnp.dot(nbuf[rows, :], gathered_rows(buf, c), preferred_element_type=F32)
         raised = jnp.maximum(raised * up_scale[:, j * COLS : (j + 1) * COLS], 0.0)
-        vn[rows, :] = (raised * raised).astype(BF)
+        if j < 3:
+            vn[rows, :] = (raised * raised).astype(BF)
+        else:
+            both_hid[lane, rows, :] = (raised * raised).astype(BF)
+            block = both_hid.at[lane, pl.ds(i * MB, MB)]
+            exchange(block, block, 6 + i, f"hid{i}")
 
     def job_dn(j, i):
         c = 4 + 2 * j
@@ -413,17 +462,52 @@
             span = slice((q % 2) * COLS, (q % 2 + 1) * COLS)
             term = dot_nt(vn[rows, :], gathered_rows(buf, c, q * 8, 8))
             acc[q // 2, rows, span] = term if j == 0 else acc[q // 2, rows, span] + term
-
-    def last_down(half, i):
+        if j == 2:
+            send_terms(i)
+
+    own, other = lane, 1 - lane
+    own_cols = pl.ds(pl.multiple_of(lane * HALF, HALF), HALF)
+
+    def send_terms(i):
+        for n in (2 * i, 2 * i + 1):
+            sent(f"out{n}")
+
+        def body(rows):
+            part[rows, :HALF] = acc[other, rows, :].astype(BF)
+
+        in_rows(i * MB, MB, EB, body, AT_ONCE)
+        block = pl.ds(i * MB, MB)
+        exchange(part.at[block, pl.ds(0, HALF)], terms_in.at[block], 8 + i, f"terms{i}")
+
+    def last_rows(half, first, count):
+        return jnp.concatenate(
+            [
+                buf[LAST, r, place(order_of(LAST, r), half * 16 + s)]
+                for s in range(first, first + count)
+                for r in range(PARTS)
+            ],
+            axis=0,
+        )
+
+    def last_down(i):
         rows = slice(i * MB, (i + 1) * MB)
+        power = None
         for q in range(2):
             span = slice(q * COLS, (q + 1) * COLS)
-            term = dot_nt(vn[rows, :], rows_of_half(buf, NCH - 1, half, q * 8, 8))
-            yield rows, span, (acc[half, rows, span] + term).astype(BF)
+            scale = scales[1:2, pl.ds(pl.multiple_of(lane * HALF + q * COLS, COLS), COLS)]
+            term = dot_nt(both_hid[0, rows, :], last_rows(0, q * 8, 8))
+            term = term + dot_nt(both_hid[1, rows, :], last_rows(1, q * 8, 8))
+            value = (acc[own, rows, span] + terms_in[rows, span].astype(F32) + term) * scale
+            acc[own, rows, span] = value
+            square = jnp.sum(value * value, axis=1, keepdims=True)
+            power = square if q == 0 else power + square
+        stats[1, rows, :] = jnp.broadcast_to(power, (MB, 128))
+        block = pl.ds(i * MB, MB)
+        exchange(stats.at[1, block], stats_in.at[1, block], 10 + i, f"power{i}")
 
     def job(name):
         kind, index = name.rstrip("0123456789"), [int(n) for n in name[len(name.rstrip("0123456789")) :]]
-        {"xn": job_xn, "u": job_u, "v": job_v, "mix": job_mix, "out": job_out, "mid": job_mid, "up": job_up, "dn": job_dn}[kind](*index)
+        {"xn": job_xn, "u": job_u, "v": job_v, "vn": job_vn, "mix": job_mix, "out": job_out, "mid": job_mid, "up": job_up, "dn": job_dn}[kind](*index)
 
     send_scales(0)
     turns = {50: 1, 90: 2, 120: 3, 150: 4, 165: 5}
@@ -440,30 +524,14 @@
                 job(name)
         else:
             c, k, r = code // 20, (code // 4) % 5, code % 4
-            if k:
+            if c == LAST and k == 0:
+                first_of_last(r)
+                continue
+            if c == LAST and k == 1:
+                first_of_last_arrived(r)
+            elif k:
                 arrived(c, k - 1, r)
             send(c, k, r)
-
-    for i in range(NRB):
-        sent(f"out{i}")
-    chunk(NCH - 1)
-    own, other = lane, 1 - lane
-    for i in range(2):
-        for rows, span, value in last_down(other, i):
-            part[rows, span] = value
-        for n in (2 * i, 2 * i + 1):
-            block = pl.ds(n * RB, RB)
-            exchange(part.at[block, pl.ds(0, HALF)], terms_in.at[block], 6 + n, f"terms{n}")
-    for i in range(2):
-        for rows, span, value in last_down(own, i):
-            acc[own, rows, span] = value.astype(F32)
-    own_cols = pl.ds(pl.multiple_of(lane * HALF, HALF), HALF)
-
-    def add_up(rows):
-        value = (acc[own, rows, :] + terms_in[rows, :].astype(F32)) * scales[1:2, own_cols]
-        acc[own, rows, :] = value
-        power = jnp.sum(value * value, axis=1, keepdims=True)
-        stats[1, rows, :] = jnp.broadcast_to(power, (EB, 128))
 
     def finish(rows):
         power = stats[1, rows, 0:1] + stats_in[1, rows, 0:1]
@@ -471,19 +539,25 @@
         value = acc[own, rows, :] * inv * gain_last[:, own_cols]
         result[rows, :] = (xfull[lane, rows, :].astype(F32) + value).astype(BF)
 
-    for i in range(NRB):
+    for i in range(2):
+        received(f"hid{i}")
         received(f"terms{i}")
-        in_rows(i * RB, RB, EB, add_up, AT_ONCE)
-        block = pl.ds(i * RB, RB)
-        exchange(stats.at[1, block], stats_in.at[1, block], 10 + i, f"power{i}")
-    for i in range(NRB):
+    chunk(LAST)
+    for i in range(2):
+        last_down(i)
+    for i in range(2):
         received(f"power{i}")
-        in_rows(i * RB, RB, EB, finish, AT_ONCE)
+        in_rows(i * MB, MB, EB, finish, AT_ONCE)
     for copy in pending.values():
         copy.wait_send()
     for c in range(NCH):
         block = buf.at[c, :, pl.ds(0, 31)]
         pltpu.make_async_copy(block, block, send_sem.at[c]).wait()
+    @pl.when(crossed == 1)
+    def _():
+        for r in range(PARTS):
+            pltpu.make_async_copy(stage.at[r], stage.at[r], first_send.at[r]).wait()
+
     for k in range(STEPS):
         block = sbuf.at[pl.ds(0, 1 << k)]
         pltpu.make_async_copy(block, block, s_send.at[k]).wait()
@@ -528,6 +602,8 @@
             pltpu.VMEM((ROWS, WIDTH), BF),
             pltpu.VMEM((2, ROWS, HALF), F32),
             pltpu.VMEM((ROWS, COLS), BF),
+            pltpu.VMEM((2, ROWS, COLS), BF),
+            pltpu.VMEM((PARTS, TILE, COLS), BF),
             pltpu.VMEM((ROWS, COLS), BF),
             pltpu.VMEM((ROWS, WIDTH), BF),
             pltpu.VMEM((ROWS, WIDTH), BF),
@@ -537,11 +613,13 @@
             dma((NCH + 1,)),
             dma((NCH,)),
             dma((NCH, STEPS, PARTS)),
+            dma((PARTS,)),
+            dma((3, PARTS)),
             dma((STEPS,)),
             dma((STEPS,)),
             dma((3,)),
-            dma((14,)),
-            dma((14,)),
+            dma((12,)),
+            dma((12,)),
         ],
         compiler_params=pltpu.CompilerParams(
             collective_id=0, has_side_effects=True, vmem_limit_bytes=VMEM_LIMIT

time: 104 us -> 104 us (level)
  no operation moved by 1% of the time
where the time goes in v4:
time: 104 us; the launch traced here: 103 us
  Pallas kernels  102 us (98%)
  local copies, waits for them, and re-layouts  1.32 us (1%)
    pallas_call x1, Pallas kernels, local(): pl.pallas_call(kernel, out_shape=pltpu.VMEM((ROWS, HALF), BF), in_specs=[...  102 us

profile of v4, /device:TPU:1, one launch (start us, length us, event | category | flops | bytes accessed | tf_op | source)
XLA Modules:
  0.0 103.4 jit_solution(16363785112801422371)
XLA Ops:
  0.0 102.1 %shard_map.172 = bf16[1024,1024]{1,0:T(8,128)(2,1)S(1)} custom-call(f32[64,512]{1,0:T(8,128)} %u_weight.1, f32[64,512]{1,0:T(8,128)} %v_weight.1, f32[64,512]{1,0:T(8,128)} %bitcast.13, f32[64,2048]{1,0:T(8,128)} %up_weight.1, f32[64,2048]{1,0:T(8,128)} %bitcast.12, bf16[1024,1024]{1,0:T(8,128)(2,1)} %resid.1, f32[8,128,128]{2,1,0:T(8,128)} %mix_matrix.1, ...), custom_call_target="tpu_custom_call" | custom-call | tf_op jit(solution)/shard_map/pallas_call | solution.py:590
  102.1 1.3 %copy.20 = bf16[1024,1024]{1,0:T(8,128)(2,1)} copy(bf16[1024,1024]{1,0:T(8,128)(2,1)S(1)} %shard_map.172) | data formatting | bytes 4194304

commit v5 on v4

--- a/solution.py
+++ b/solution.py
@@ -25,7 +25,7 @@
 NRB = ROWS // RB
 MB = 512
 EB = 32
-AT_ONCE = 2
+AT_ONCE = 4
 VMEM_LIMIT = 58 * 1024 * 1024
 
 CROSSINGS = [

time: 104 us -> 103 us (level)
  no operation moved by 1% of the time
where the time goes in v5:
time: 103 us
  Pallas kernels  101 us (98%)
  local copies, waits for them, and re-layouts  1.32 us (1%)
    pallas_call x1, Pallas kernels, local(): pl.pallas_call(kernel, out_shape=pltpu.VMEM((ROWS, HALF), BF), in_specs=[...  101 us

profile of v5, /device:TPU:1, one launch (start us, length us, event | category | flops | bytes accessed | tf_op | source)
XLA Modules:
  0.0 102.8 jit_solution(13647564651292675611)
XLA Ops:
  0.0 101.5 %shard_map.172 = bf16[1024,1024]{1,0:T(8,128)(2,1)S(1)} custom-call(f32[64,512]{1,0:T(8,128)} %u_weight.1, f32[64,512]{1,0:T(8,128)} %v_weight.1, f32[64,512]{1,0:T(8,128)} %bitcast.13, f32[64,2048]{1,0:T(8,128)} %up_weight.1, f32[64,2048]{1,0:T(8,128)} %bitcast.12, bf16[1024,1024]{1,0:T(8,128)(2,1)} %resid.1, f32[8,128,128]{2,1,0:T(8,128)} %mix_matrix.1, ...), custom_call_target="tpu_custom_call" | custom-call | tf_op jit(solution)/shard_map/pallas_call | solution.py:590
  101.5 1.3 %copy.20 = bf16[1024,1024]{1,0:T(8,128)(2,1)} copy(bf16[1024,1024]{1,0:T(8,128)(2,1)S(1)} %shard_map.172) | data formatting | bytes 4194304
